TPU v7x, 32 devices: a whole 2x2x4 slice. The times are simulated.
32 devices in a mesh: fs: 8 (over z, y), tp: 4 (over x, core).
Axes of the slice: x: 2, y: 2, z: 4, core: 2. Of those that a mesh axis runs over, the one named last changes fastest.
Arguments:
- later_input: bfloat16 [4096, 2048], P(('fs', 'tp')), may hold values from -6 to 6
- earlier_input: bfloat16 [4096, 2048], P('fs'), may hold values from -6 to 6
- earlier_hidden: bfloat16 [4096, 4096], P('fs', 'tp'), may hold values from -6 to 6
- cotangent: bfloat16 [4096, 2048], P('fs'), may hold values from -6 to 6
- up_weight: bfloat16 [2048, 4096], P('fs', 'tp'), may hold values from -0.125 to 0.125
- down_weight: bfloat16 [4096, 2048], P(('tp', 'fs')), may hold values from -0.09375 to 0.09375
- up_sum: float32 [2048, 4096], P('fs', 'tp'), may hold values from -4 to 4
- down_sum: float32 [4096, 2048], P(('tp', 'fs')), may hold values from -4 to 4
Outputs:
- later_output: bfloat16 [4096, 2048], P(('fs', 'tp'))
- later_hidden: bfloat16 [4096, 4096], P('fs', 'tp')
- earlier_grad: bfloat16 [4096, 2048], P(('fs', 'tp'))
- up_sum_next: float32 [2048, 4096], P('fs', 'tp')
- down_sum_next: float32 [4096, 2048], P(('tp', 'fs'))
All inputs are finite; a program needn't handle non-finite values.
Results may differ from a plain program's by a relative error of at most 0.0095.
Values may be sent and summed in bfloat16 or wider, within the bound.
A program may use at most 128 MiB of HBM per device.

v0:
```python
import functools

import jax
import jax.numpy as jnp
from jax import lax
from jax.experimental import pallas as pl
from jax.experimental.pallas import tpu as pltpu
from jax.sharding import PartitionSpec as P

F32, BF16 = jnp.float32, jnp.bfloat16
MESH = pl.DeviceIdType.MESH
LANES = 128
VMEM_BYTES = 67_043_328


def dot(a, b, ca=1, cb=0):
    return lax.dot_general(a, b, (((ca,), (cb,)), ((), ())), preferred_element_type=F32)


def loop(n, body):
    def step(i, carry):
        body(i)
        return carry

    lax.fori_loop(0, n, step, 0)


def squared(h):
    lifted = jnp.maximum(h.astype(F32), 0.0)
    return (lifted * lifted).astype(BF16)


def both(a, b):
    return jnp.logical_and(a, b)


class Wire:
    def __init__(self, send, recv, local):
        self.send, self.recv, self.local = send, recv, local
        self.n_remote = self.n_local = 0
        self.open = []

    def slot(self):
        self.n_remote += 1
        return self.n_remote - 1

    def remote(self, src, dst, device, slot=None):
        i = self.slot() if slot is None else slot
        return pltpu.make_async_remote_copy(
            src_ref=src, dst_ref=dst, send_sem=self.send.at[i], recv_sem=self.recv.at[i],
            device_id=device, device_id_type=MESH,
        )

    def start(self, copy, when=None):
        if when is None:
            copy.start()
        else:
            pl.when(when)(copy.start)
        self.open.append((copy, when))

    def copy(self, src, dst):
        i = self.n_local
        self.n_local += 1
        made = pltpu.make_async_copy(src, dst, self.local.at[i])
        made.start()
        return made

    def drain(self):
        for copy, when in self.open:
            if when is None:
                copy.wait_send()
            else:
                pl.when(when)(copy.wait_send)


class Line:
    def __init__(self, wire, full, rows, own, z, n, left, right):
        self.wire, self.z, self.n = wire, z, n
        self.right, self.left = {}, {}

        def block(i):
            return full.at[pl.ds(pl.multiple_of(lax.rem(i + n, n) * rows, rows), rows)]

        for r in range(1, n):
            src = own if r == 1 else block(z - r + 1)
            self.right[r] = wire.remote(src, block(z - r + 1), right)
            src = own if r == 1 else block(z + r - 1)
            self.left[r] = wire.remote(src, block(z + r - 1), left)

    def begin(self):
        self.wire.start(self.right[1], self.z < self.n - 1)
        self.wire.start(self.left[1], self.z > 0)

    def wave(self, r):
        z, n = self.z, self.n
        pl.when(z >= r)(self.right[r].wait_recv)
        if r < n - 1:
            self.wire.start(self.right[r + 1], both(z >= r, z < n - 1))
        pl.when(z <= n - 1 - r)(self.left[r].wait_recv)
        if r < n - 1:
            self.wire.start(self.left[r + 1], both(z <= n - 1 - r, z > 0))


class Sums:
    def __init__(self, wire, part, inbox, relayed, rows, z, n, left, right):
        self.wire, self.part, self.inbox, self.relayed = wire, part, inbox, relayed
        self.rows, self.z, self.n = rows, z, n
        self.seed, self.pass_on = {}, {}
        for way, device in ((0, right), (1, left)):
            for m in range(n - 1):
                slot = wire.slot()
                dst = inbox.at[way, m]
                self.seed[way, m] = wire.remote(part.at[self.span(way, m)], dst, device, slot)
                if m < n - 2:
                    self.pass_on[way, m] = wire.remote(relayed.at[way, m], dst, device, slot)

    def span(self, way, m, lo=0, size=None):
        ahead = self.z + 1 + m if way == 0 else self.z - 1 - m
        base = lax.rem(ahead + 2 * self.n, self.n) * self.rows
        size = self.rows if size is None else size
        return pl.ds(pl.multiple_of(base + lo, size), size)

    def seeds(self, ms):
        for m in ms:
            self.wire.start(self.seed[0, m], self.z == 0)
            self.wire.start(self.seed[1, m], self.z == self.n - 1)

    def relay(self, m):
        z, n = self.z, self.n
        tile = self.rows // 4
        for way in (0, 1):
            if way == 0:
                when = both(z >= 1, z + 1 + m <= n - 1)
            else:
                when = both(z <= n - 2, z - 1 - m >= 0)

            def add(way=way):
                self.seed[way, m + 1].wait_recv()

                def body(i):
                    lo = pl.multiple_of(i * tile, tile)
                    mine = self.part[self.span(way, m, lo, tile), :].astype(F32)
                    came = self.inbox[way, m + 1, pl.ds(lo, tile), :].astype(F32)
                    self.relayed[way, m, pl.ds(lo, tile), :] = (mine + came).astype(BF16)

                loop(4, body)

            pl.when(when)(add)
            self.wire.start(self.pass_on[way, m], when)

    def final(self, out, order, tile):
        z, n = self.z, self.n
        pl.when(z >= 1)(self.seed[0, 0].wait_recv)
        pl.when(z <= n - 2)(self.seed[1, 0].wait_recv)
        up, down = (z >= 1).astype(F32), (z <= n - 2).astype(F32)
        base = z * self.rows

        def body(i):
            lo = pl.multiple_of(order(i) * tile, tile)
            rows = pl.ds(lo, tile)
            mine = self.part[pl.ds(pl.multiple_of(base + lo, tile), tile), :].astype(F32)
            first = jnp.where(z >= 1, self.inbox[0, 0, rows, :].astype(F32), 0.0)
            second = jnp.where(z <= n - 2, self.inbox[1, 0, rows, :].astype(F32), 0.0)
            out[rows, :] = mine + first + second

        loop(self.rows // tile, body)


class Plane:
    def __init__(self, wire, bufs, k, at, peers):
        part, in_a, to_b, in_b, to_c, in_c = (buf.at[k] for buf in bufs)
        self.part, self.in_a, self.to_b, self.in_b, self.to_c, self.in_c = (
            part, in_a, to_b, in_b, to_c, in_c
        )
        self.wire, self.at = wire, at
        x, y, c = at
        self.a = wire.remote(part.at[1 - c], in_a, peers[2])
        self.b = wire.remote(to_b, in_b, peers[0])
        self.c = wire.remote(to_c, in_c, peers[1])

    def begin(self):
        self.wire.start(self.a)

    def second(self):
        x, y, c = self.at
        self.a.wait_recv()
        for j in (0, 1):
            total = self.part[c, 1 - x, j].astype(F32) + self.in_a[1 - x, j].astype(F32)
            self.to_b[j] = total.astype(BF16)
        self.wire.start(self.b)

    def mine(self, j):
        x, y, c = self.at
        return (
            self.part[c, x, j].astype(F32) + self.in_a[x, j].astype(F32) + self.in_b[j].astype(F32)
        )

    def third(self):
        x, y, c = self.at
        self.b.wait_recv()
        self.to_c[...] = self.mine(1 - y).astype(BF16)
        self.wire.start(self.c)

    def last(self, out, columns):
        x, y, c = self.at
        self.c.wait_recv()
        out[:, columns] = (self.mine(y) + self.in_c[...].astype(F32)).astype(BF16)


def layer(
    n, later_in, earlier_in, hidden, cot, up, down,
    out_o, lh_o, eg_o, gu_o, gd_o,
    c_all, e_all, x_all, h_all, act_t, pg, up_full, down_full, gd_part, gu_part,
    gd_in, gd_relay, gu_in, gu_relay, swap_out, swap_in, lh, act_l,
    part, in_a, to_b, in_b, to_c, in_c, eg_fin, out_fin, gd_fin, gu_fin, gu_out,
    send, recv, local,
):
    fs, tp = lax.axis_index("fs"), lax.axis_index("tp")
    z, y = fs // 2, fs % 2
    x, c = tp // 2, tp % 2
    py, px, pc = (fs + 1 - 2 * y, tp), (fs, tp + 2 - 4 * x), (fs, tp + 1 - 2 * c)
    left, right = (lax.rem(fs + 2 * n - 2, 2 * n), tp), (lax.rem(fs + 2, 2 * n), tp)

    group, width = earlier_in.shape
    block = later_in.shape[0]
    hb = down.shape[0]
    half = n * hb
    up_rows = up.shape[0]
    chunk = 2 * up_rows
    wire = Wire(send, recv, local)

    def cols(i, parity):
        return pl.ds(pl.multiple_of((2 * i + parity) * hb, hb), hb)

    def strip(i):
        return pl.ds(i * hb, hb)

    def rows_of(parity, q):
        return pl.ds(pl.multiple_of(parity * group + q * block, block), block)

    def half_of(parity):
        return pl.ds(pl.multiple_of(parity * group, group), group)

    barrier = pltpu.get_barrier_semaphore()

    def greet(device):
        pl.semaphore_signal(barrier, inc=1, device_id=device, device_id_type=MESH)

    for device in (py, px, pc):
        greet(device)
    pl.when(z > 0)(lambda: greet(left))
    pl.when(z < n - 1)(lambda: greet(right))

    own_h = [wire.copy(hidden.at[:, cols(i, y)], h_all.at[half_of(y), strip(i)]) for i in range(n)]
    my_rows = pl.ds(pl.multiple_of(fs * up_rows, up_rows), up_rows)
    own_up = [wire.copy(up.at[:, cols(i, y)], up_full.at[my_rows, strip(i)]) for i in range(n)]
    own_c = wire.copy(cot, c_all.at[half_of(y)])
    own_down = wire.copy(down, down_full.at[pl.ds(pl.multiple_of(z * hb, hb), hb)])
    own_e = wire.copy(earlier_in, e_all.at[half_of(y)])
    own_x = wire.copy(later_in, x_all.at[rows_of(y, tp)])

    pl.semaphore_wait(barrier, 3 + (z > 0).astype(jnp.int32) + (z < n - 1).astype(jnp.int32))

    def spread(whole, source, src_rows):
        there = whole.at[rows_of(y, tp)]
        came = whole.at[rows_of(1 - y, tp)]
        beside = whole.at[rows_of(1 - y, tp + 2 - 4 * x)]
        return (
            wire.remote(source.at[src_rows], there, py),
            wire.remote(came, came, px),
            wire.remote(came, came, pc),
            wire.remote(beside, beside, pc),
        )

    quarter = pl.ds(pl.multiple_of(tp * block, block), block)
    downs = Line(wire, down_full, hb, down, z, n, left, right)
    up_block = up_full.at[pl.ds(pl.multiple_of(z * chunk, chunk), chunk)]
    ups = Line(wire, up_full, chunk, up_block, z, n, left, right)
    c_y, c_x, c_c, c_xc = spread(c_all, cot, quarter)
    e_y, e_x, e_c, e_xc = spread(e_all, earlier_in, quarter)
    x_y, x_x, x_c, x_xc = spread(x_all, later_in, pl.ds(0, block))
    mine_x = x_all.at[rows_of(y, tp)]
    beside_x = x_all.at[rows_of(y, tp + 2 - 4 * x)]
    x_own_x = wire.remote(later_in, mine_x, px)
    x_own_c = wire.remote(later_in, mine_x, pc)
    x_own_xc = wire.remote(beside_x, beside_x, pc)
    up_y = [
        wire.remote(up.at[:, cols(i, 1 - y)], up_full.at[my_rows, strip(i)], py) for i in range(n)
    ]
    h_y = [
        wire.remote(hidden.at[:, cols(i, 1 - y)], h_all.at[half_of(y), strip(i)], py)
        for i in range(n)
    ]

    downs.begin()
    wire.start(c_y)
    for copy in up_y + h_y:
        wire.start(copy)
    wire.start(e_y)
    wire.start(x_y)
    wire.start(x_own_x)
    wire.start(x_own_c)

    gds = Sums(wire, gd_part, gd_in, gd_relay, hb, z, n, left, right)
    gus = Sums(wire, gu_part, gu_in, gu_relay, chunk, z, n, left, right)
    bufs = (part, in_a, to_b, in_b, to_c, in_c)
    planes = [Plane(wire, bufs, k, (x, y, c), (px, py, pc)) for k in range(2 * n)]
    egs, outs = planes[:n], planes[n:]

    def activate(parity):
        def body(i):
            rows = rows_of(parity, i)
            act_t[:, rows] = squared(h_all[rows, :]).T

        loop(group // block, body)

    for copy in own_h:
        copy.wait()
    activate(y)

    downs.wave(1)
    c_y.wait_recv()
    wire.start(c_x)
    wire.start(c_c)
    for copy in own_up:
        copy.wait()
    for copy in up_y:
        copy.wait_recv()
    ups.begin()
    if n > 2:
        downs.wave(2)
    c_x.wait_recv()
    wire.start(c_xc)
    for copy in h_y:
        copy.wait_recv()
    activate(1 - y)
    c_c.wait_recv()
    c_xc.wait_recv()
    own_c.wait()

    tile = min(256, chunk)

    def gd_body(i):
        columns = pl.ds(pl.multiple_of(i * tile, tile), tile)
        gd_part[:, columns] = dot(act_t[...], c_all[:, columns]).astype(BF16)

    loop(width // tile, gd_body)
    gds.seeds(range(n - 2, 0, -1))

    for r in range(3, n):
        downs.wave(r)
    own_down.wait()

    slope_rows = min(256, 2 * group)

    def pg_body(i):
        rows = pl.ds(pl.multiple_of(i * slope_rows, slope_rows), slope_rows)
        lifted = jnp.maximum(h_all[rows, :].astype(F32), 0.0)
        pg[rows, :] = (2.0 * dot(c_all[rows, :], down_full[...], 1, 1) * lifted).astype(BF16)

    loop(2 * group // slope_rows, pg_body)

    e_y.wait_recv()
    wire.start(e_x)
    wire.start(e_c)

    def store_part(k, parity, value):
        for q in range(4):
            part[k, q % 2, q // 2, parity] = value[q * block : (q + 1) * block].astype(BF16)

    def column_block(k):
        where = 0
        for i in range(n):
            order = sorted(range(n), key=lambda b: (abs(b - i), b))
            where = where + jnp.where(z == i, order[k], 0)
        return pl.ds(pl.multiple_of(where * chunk, chunk), chunk)

    def eg_chunk(k):
        wide = column_block(k)

        def body(parity):
            store_part(k, parity, dot(pg[half_of(parity), :], up_full[wide, :], 1, 1))

        loop(2, body)
        egs[k].begin()

    def out_chunk(k):
        wide = pl.ds(k * chunk, chunk)

        def body(parity):
            store_part(n + k, parity, dot(act_l[half_of(parity), :], down_full[:, wide]))

        loop(2, body)
        outs[k].begin()

    eg_chunk(0)
    for m in range(n - 3, 0, -1):
        gds.relay(m)
    ups.wave(1)
    egs[0].second()
    eg_chunk(1)
    e_x.wait_recv()
    wire.start(e_xc)
    e_c.wait_recv()
    e_xc.wait_recv()
    own_e.wait()

    def gu_body(i):
        wide = pl.ds(pl.multiple_of(i * tile, tile), tile)
        gu_part[wide, :] = dot(e_all[:, wide], pg[...], 0, 0).astype(BF16)

    loop(width // tile, gu_body)
    gus.seeds(range(n - 2, -1, -1))
    gds.seeds([0])

    x_y.wait_recv()
    wire.start(x_x)
    wire.start(x_c)
    egs[0].third()
    egs[1].second()
    for r in range(2, n - 1):
        ups.wave(r)
        eg_chunk(r)
    if n > 2:
        gds.relay(0)
    x_own_x.wait_recv()
    wire.start(x_own_xc)
    egs[1].third()
    for r in range(2, n - 1):
        egs[r].second()
    x_x.wait_recv()
    wire.start(x_xc)
    for copy in (x_own_c, x_c, x_own_xc, x_xc):
        copy.wait_recv()
    own_x.wait()
    for r in range(2, n - 1):
        egs[r].third()

    if n > 2:
        ups.wave(n - 1)
        eg_chunk(n - 1)

    def lh_body(parity):
        rows = half_of(parity)

        def body(i):
            at = pl.ds(pl.multiple_of(parity * group + i * slope_rows, slope_rows), slope_rows)
            h = dot(x_all[at, :], up_full[...]).astype(BF16)
            lh[at, :] = h
            act_l[at, :] = squared(h)

        loop(group // slope_rows, body)
        return rows

    theirs = lh_body(1 - y)
    lh_y = [
        wire.remote(lh.at[theirs, strip(i)], lh_o.at[:, cols(i, y)], py) for i in range(n)
    ]
    for copy in lh_y:
        wire.start(copy)
    egs[n - 1].second()
    ours = lh_body(y)
    lh_mine = [wire.copy(lh.at[ours, strip(i)], lh_o.at[:, cols(i, y)]) for i in range(n)]
    for k in range(n):
        out_chunk(k)
        if k:
            outs[k - 1].second()
    outs[n - 1].second()
    for m in range(n - 3, -1, -1):
        gus.relay(m)
    egs[n - 1].third()
    for k in range(n):
        outs[k].third()

    gds.final(gd_fin, lambda i: i, hb // 4)
    gd_done = wire.copy(gd_fin, gd_o)
    per = up_rows // (chunk // 4)
    gus.final(gu_fin, lambda i: lax.rem(i + (1 - y) * per, 2 * per), chunk // 4)
    swap_out[...] = gu_fin[pl.ds(pl.multiple_of((1 - y) * up_rows, up_rows), up_rows), :].astype(BF16)
    swap = wire.remote(swap_out, swap_in, py)
    wire.start(swap)
    for k in range(n):
        egs[k].last(eg_fin, column_block(k))
    eg_done = wire.copy(eg_fin, eg_o)
    for k in range(n):
        outs[k].last(out_fin, pl.ds(k * chunk, chunk))
    out_done = wire.copy(out_fin, out_o)
    swap.wait_recv()
    for i in range(n):
        gu_out[:, cols(i, y)] = gu_fin[pl.ds(pl.multiple_of(y * up_rows, up_rows), up_rows), strip(i)]
        gu_out[:, cols(i, 1 - y)] = swap_in[:, strip(i)].astype(F32)
    gu_done = wire.copy(gu_out, gu_o)
    for copy in lh_y:
        copy.wait_recv()
    for copy in lh_mine + [gd_done, eg_done, out_done, gu_done]:
        copy.wait()
    wire.drain()


def fused(n, later_in, earlier_in, hidden, cot, up, down):
    group, width = earlier_in.shape
    block, hb, up_rows = later_in.shape[0], down.shape[0], up.shape[0]
    half, tokens, chunk = n * hb, 2 * group, 2 * up_rows
    any_space = pl.BlockSpec(memory_space=pl.ANY)
    shapes = (
        jax.ShapeDtypeStruct(later_in.shape, BF16),
        jax.ShapeDtypeStruct(hidden.shape, BF16),
        jax.ShapeDtypeStruct(later_in.shape, BF16),
        jax.ShapeDtypeStruct(up.shape, F32),
        jax.ShapeDtypeStruct(down.shape, F32),
    )
    vm = pltpu.VMEM
    scratch = [
        vm((tokens, width), BF16), vm((tokens, width), BF16), vm((tokens, width), BF16),
        vm((tokens, half), BF16), vm((half, tokens), BF16), vm((tokens, half), BF16),
        vm((width, half), BF16), vm((half, width), BF16),
        vm((half, width), BF16), vm((width, half), BF16),
        vm((2, n - 1, hb, width), BF16), vm((2, max(n - 2, 1), hb, width), BF16),
        vm((2, n - 1, chunk, half), BF16), vm((2, max(n - 2, 1), chunk, half), BF16),
        vm((up_rows, half), BF16), vm((up_rows, half), BF16),
        vm((tokens, half), BF16), vm((tokens, half), BF16),
        vm((2 * n, 2, 2, 2, block, chunk), BF16), vm((2 * n, 2, 2, block, chunk), BF16),
        vm((2 * n, 2, block, chunk), BF16), vm((2 * n, 2, block, chunk), BF16),
        vm((2 * n, block, chunk), BF16), vm((2 * n, block, chunk), BF16),
        vm((block, width), BF16), vm((block, width), BF16),
        vm((hb, width), F32), vm((chunk, half), F32), vm(up.shape, F32),
    ]
    remote_copies = 8 * (n - 1) + 15 + 3 * n + 6 * n + 1
    local_copies = 3 * n + 8
    return pl.pallas_call(
        functools.partial(layer, n),
        out_shape=shapes,
        in_specs=[any_space] * 6,
        out_specs=(any_space,) * 5,
        scratch_shapes=scratch + [
            pltpu.SemaphoreType.DMA((remote_copies,)),
            pltpu.SemaphoreType.DMA((remote_copies,)),
            pltpu.SemaphoreType.DMA((local_copies,)),
        ],
        compiler_params=pltpu.CompilerParams(
            collective_id=0, has_side_effects=True, vmem_limit_bytes=VMEM_BYTES
        ),
        name="layer",
    )(later_in, earlier_in, hidden, cot, up, down)


def portable(later_in, earlier_in, hidden, cot, up, down):
    def split_sum(partial, axis):
        return lax.psum_scatter(partial.astype(F32), axis, scatter_dimension=0, tiled=True)

    up_full = lax.all_gather(up, "fs", axis=0, tiled=True)
    down_full = lax.all_gather(down, "fs", axis=0, tiled=True)
    rows = lax.all_gather(later_in, "tp", axis=0, tiled=True)
    lifted = jnp.maximum(hidden.astype(F32), 0.0)
    gd = split_sum(dot(squared(hidden), cot, 0, 0), "fs")
    pre = (2.0 * dot(cot, down_full, 1, 1) * lifted).astype(BF16)
    gu = split_sum(dot(earlier_in, pre, 0, 0), "fs")
    eg = split_sum(dot(pre, up_full, 1, 1).astype(BF16), "tp").astype(BF16)
    later_hidden = dot(rows, up_full).astype(BF16)
    out = split_sum(dot(squared(later_hidden), down_full).astype(BF16), "tp").astype(BF16)
    return out, later_hidden, eg, gu, gd


def solution(mesh):
    n_fs, n_tp = mesh.shape["fs"], mesh.shape["tp"]

    def shards(
        later_input, earlier_input, earlier_hidden, cotangent, up_weight, down_weight, up_sum, down_sum
    ):
        scale = float(earlier_input.shape[0] * n_fs) ** (-0.5)
        args = (later_input, earlier_input, earlier_hidden, cotangent, up_weight, down_weight)
        planes = n_fs // 2
        fits = (
            n_tp == 4 and n_fs % 2 == 0 and 2 < planes <= 4
            and down_weight.shape[0] % LANES == 0 and up_weight.shape[0] % LANES == 0
            and later_input.shape[0] % LANES == 0
        )
        out, later_hidden, eg, gu, gd = fused(planes, *args) if fits else portable(*args)
        return out, later_hidden, eg, up_sum + scale * gu, down_sum + scale * gd

    in_specs = (
        P(("fs", "tp"), None), P("fs", None), P("fs", "tp"), P("fs", None),
        P("fs", "tp"), P(("tp", "fs"), None), P("fs", "tp"), P(("tp", "fs"), None),
    )
    out_specs = (
        P(("fs", "tp"), None), P("fs", "tp"), P(("fs", "tp"), None),
        P("fs", "tp"), P(("tp", "fs"), None),
    )
    return jax.shard_map(shards, mesh=mesh, in_specs=in_specs, out_specs=out_specs, check_vma=False)
```

profile of v0, /device:TPU:0, one launch (start us, length us, event | category | flops | bytes accessed | tf_op | source)
XLA Modules:
  0.0 152.6 jit_solution(11249470577505402459)
XLA Ops:
  0.6 145.4 %layer.1 = (bf16[128,2048]{1,0:T(8,128)(2,1)}, bf16[512,1024]{1,0:T(8,128)(2,1)}, bf16[128,2048]{1,0:T(8,128)(2,1)}, f32[256,1024]{1,0:T(8,128)}, f32[128,2048]{1,0:T(8,128)}) custom-call(bf16[128,2048]{1,0:T(8,128)(2,1)} %later_in.1, bf16[512,2048]{1,0:T(8,128)(2,1)} %earlier_in.1, bf16[512,1024]{1,0:T(8,128)(2,1)} %hidden.1, bf16[512,2048]{1,0:T(8,128)(2,1)} %cot.1, ...), custom_call_target="tpu_custom_call" | custom-call | tf_op jit(solution)/shard_map/layer/pallas_call | solution.py:530
  146.1 0.0 copy-start
  146.1 0.0 copy-start.1
  146.1 2.9 %multiply_add_fusion.1 = f32[256,1024]{1,0:T(8,128)} fusion(f32[256,1024]{1,0:T(8,128)} %param.14, f32[256,1024]{1,0:T(8,128)} %get-tuple-element.13), kind=kLoop, calls=%fused_computation.1 | loop fusion | flops 524288 | bytes 3145728 | tf_op jit(solution)/shard_map/add | solution.py:579
  149.0 0.0 copy-done
  149.0 0.0 copy-done.1
  149.0 0.0 copy-start.4
  149.0 0.0 copy-start.2
  149.0 1.1 multiply_add_fusion
  150.1 0.0 copy-done.4
  150.1 0.0 copy-start.3
  150.1 0.8 copy.16
  150.9 0.0 copy-done.2
  150.9 1.0 copy.17
  151.8 0.0 copy-done.3
  151.8 0.8 copy.18
Async XLA Ops:
  146.1 2.9 %copy-start = (f32[128,2048]{1,0:T(8,128)S(1)}, f32[128,2048]{1,0:T(8,128)}, u32[]{:S(2)}) copy-start(f32[128,2048]{1,0:T(8,128)} %param.15) | copy-start | bytes 3145732
  146.1 2.9 %copy-start.1 = (f32[128,2048]{1,0:T(8,128)S(1)}, f32[128,2048]{1,0:T(8,128)}, u32[]{:S(2)}) copy-start(f32[128,2048]{1,0:T(8,128)} %get-tuple-element.14) | copy-start | bytes 3145732
  149.0 1.1 copy-start.4
  149.0 1.9 %copy-start.2 = (bf16[512,1024]{1,0:T(8,128)(2,1)S(1)}, bf16[512,1024]{1,0:T(8,128)(2,1)}, u32[]{:S(2)}) copy-start(bf16[512,1024]{1,0:T(8,128)(2,1)} %get-tuple-element.21) | copy-start | bytes 3145732
  150.1 1.8 %copy-start.3 = (bf16[128,2048]{1,0:T(8,128)(2,1)S(1)}, bf16[128,2048]{1,0:T(8,128)(2,1)}, u32[]{:S(2)}) copy-start(bf16[128,2048]{1,0:T(8,128)(2,1)} %get-tuple-element.22) | copy-start | bytes 1572868
where the time goes:
time: 153 us
  Pallas kernels  145 us (95%)
  other arithmetic  3.96 us (3%)
  local copies, waits for them, and re-layouts  2.58 us (2%)
    pallas_call x1, Pallas kernels, fused(): pl.pallas_call(functools.partial(layer, n), out_shape=shapes, in_specs=[a...  145 us
    add x2, other arithmetic, shards(): return (out, later_hidden, eg, up_sum + scale * gu, down_sum + scale * gd)  3.96 us

commit v1 on v0

--- a/solution.py
+++ b/solution.py
@@ -87,18 +87,22 @@
             src = own if r == 1 else block(z + r - 1)
             self.left[r] = wire.remote(src, block(z + r - 1), left)
 
-    def begin(self):
-        self.wire.start(self.right[1], self.z < self.n - 1)
-        self.wire.start(self.left[1], self.z > 0)
-
-    def wave(self, r):
+    def begin(self, right=True, left=True):
+        self.wire.start(self.right[1], both(self.z < self.n - 1, right))
+        self.wire.start(self.left[1], both(self.z > 0, left))
+
+    def forward(self, r):
         z, n = self.z, self.n
-        pl.when(z >= r)(self.right[r].wait_recv)
-        if r < n - 1:
-            self.wire.start(self.right[r + 1], both(z >= r, z < n - 1))
-        pl.when(z <= n - 1 - r)(self.left[r].wait_recv)
-        if r < n - 1:
-            self.wire.start(self.left[r + 1], both(z <= n - 1 - r, z > 0))
+        rightward, leftward = both(z >= r, z < n - 1), both(z <= n - 1 - r, z > 0)
+        pl.when(rightward)(self.right[r].wait_recv)
+        self.wire.start(self.right[r + 1], rightward)
+        pl.when(leftward)(self.left[r].wait_recv)
+        self.wire.start(self.left[r + 1], leftward)
+
+    def ends(self, r):
+        z, n = self.z, self.n
+        pl.when(both(z >= r, z == n - 1))(self.right[r].wait_recv)
+        pl.when(both(z <= n - 1 - r, z == 0))(self.left[r].wait_recv)
 
 
 class Sums:
@@ -167,44 +171,39 @@
 
 
 class Plane:
-    def __init__(self, wire, bufs, k, at, peers):
-        part, in_a, to_b, in_b, to_c, in_c = (buf.at[k] for buf in bufs)
-        self.part, self.in_a, self.to_b, self.in_b, self.to_c, self.in_c = (
-            part, in_a, to_b, in_b, to_c, in_c
-        )
-        self.wire, self.at = wire, at
-        x, y, c = at
-        self.a = wire.remote(part.at[1 - c], in_a, peers[2])
-        self.b = wire.remote(to_b, in_b, peers[0])
-        self.c = wire.remote(to_c, in_c, peers[1])
+    def __init__(self, wire, bufs, k, at, peers, x_first):
+        self.part, self.in_a, self.to_b, self.in_b, self.to_c, self.in_c = (b.at[k] for b in bufs)
+        self.wire, self.x_first = wire, x_first
+        x, y, self.core = at
+        self.one, self.two = (x, y) if x_first else (y, x)
+        self.a = wire.remote(self.part.at[1 - self.core], self.in_a, peers[2])
+        self.b = wire.remote(self.to_b, self.in_b, peers[0 if x_first else 1])
+        self.c = wire.remote(self.to_c, self.in_c, peers[1 if x_first else 0])
+
+    def pair(self, one, two):
+        i, j = (one, two) if self.x_first else (two, one)
+        return self.part[self.core, i, j].astype(F32) + self.in_a[i, j].astype(F32)
+
+    def mine(self, two):
+        return self.pair(self.one, two) + self.in_b[two].astype(F32)
 
     def begin(self):
         self.wire.start(self.a)
 
     def second(self):
-        x, y, c = self.at
         self.a.wait_recv()
-        for j in (0, 1):
-            total = self.part[c, 1 - x, j].astype(F32) + self.in_a[1 - x, j].astype(F32)
-            self.to_b[j] = total.astype(BF16)
+        for two in (0, 1):
+            self.to_b[two] = self.pair(1 - self.one, two).astype(BF16)
         self.wire.start(self.b)
 
-    def mine(self, j):
-        x, y, c = self.at
-        return (
-            self.part[c, x, j].astype(F32) + self.in_a[x, j].astype(F32) + self.in_b[j].astype(F32)
-        )
-
     def third(self):
-        x, y, c = self.at
         self.b.wait_recv()
-        self.to_c[...] = self.mine(1 - y).astype(BF16)
+        self.to_c[...] = self.mine(1 - self.two).astype(BF16)
         self.wire.start(self.c)
 
     def last(self, out, columns):
-        x, y, c = self.at
         self.c.wait_recv()
-        out[:, columns] = (self.mine(y) + self.in_c[...].astype(F32)).astype(BF16)
+        out[:, columns] = (self.mine(self.two) + self.in_c[...].astype(F32)).astype(BF16)
 
 
 def layer(
@@ -261,24 +260,30 @@
 
     pl.semaphore_wait(barrier, 3 + (z > 0).astype(jnp.int32) + (z < n - 1).astype(jnp.int32))
 
-    def spread(whole, source, src_rows):
-        there = whole.at[rows_of(y, tp)]
-        came = whole.at[rows_of(1 - y, tp)]
-        beside = whole.at[rows_of(1 - y, tp + 2 - 4 * x)]
-        return (
-            wire.remote(source.at[src_rows], there, py),
-            wire.remote(came, came, px),
-            wire.remote(came, came, pc),
-            wire.remote(beside, beside, pc),
-        )
-
-    quarter = pl.ds(pl.multiple_of(tp * block, block), block)
+    def spread(whole, source, first, parts):
+        size = block // parts
+
+        def sub(parity, q, i):
+            base = parity * group + q * block + i * size
+            return whole.at[pl.ds(pl.multiple_of(base, size), size)]
+
+        made = []
+        for i in range(parts):
+            there, came = sub(y, tp, i), sub(1 - y, tp, i)
+            beside = sub(1 - y, tp + 2 - 4 * x, i)
+            src = source.at[pl.ds(pl.multiple_of(first + i * size, size), size)]
+            made.append((
+                wire.remote(src, there, py), wire.remote(came, came, px),
+                wire.remote(came, came, pc), wire.remote(beside, beside, pc),
+            ))
+        return zip(*made)
+
     downs = Line(wire, down_full, hb, down, z, n, left, right)
     up_block = up_full.at[pl.ds(pl.multiple_of(z * chunk, chunk), chunk)]
     ups = Line(wire, up_full, chunk, up_block, z, n, left, right)
-    c_y, c_x, c_c, c_xc = spread(c_all, cot, quarter)
-    e_y, e_x, e_c, e_xc = spread(e_all, earlier_in, quarter)
-    x_y, x_x, x_c, x_xc = spread(x_all, later_in, pl.ds(0, block))
+    c_y, c_x, c_c, c_xc = spread(c_all, cot, tp * block, 2)
+    e_y, e_x, e_c, e_xc = spread(e_all, earlier_in, tp * block, 2)
+    x_y, x_x, x_c, x_xc = spread(x_all, later_in, 0, 2)
     mine_x = x_all.at[rows_of(y, tp)]
     beside_x = x_all.at[rows_of(y, tp + 2 - 4 * x)]
     x_own_x = wire.remote(later_in, mine_x, px)
@@ -292,20 +297,25 @@
         for i in range(n)
     ]
 
-    downs.begin()
-    wire.start(c_y)
-    for copy in up_y + h_y:
-        wire.start(copy)
-    wire.start(e_y)
-    wire.start(x_y)
-    wire.start(x_own_x)
-    wire.start(x_own_c)
-
     gds = Sums(wire, gd_part, gd_in, gd_relay, hb, z, n, left, right)
     gus = Sums(wire, gu_part, gu_in, gu_relay, chunk, z, n, left, right)
     bufs = (part, in_a, to_b, in_b, to_c, in_c)
-    planes = [Plane(wire, bufs, k, (x, y, c), (px, py, pc)) for k in range(2 * n)]
+    planes = [Plane(wire, bufs, k, (x, y, c), (px, py, pc), k >= n) for k in range(2 * n)]
     egs, outs = planes[:n], planes[n:]
+    tile = min(256, chunk)
+    slope_rows = min(256, 2 * group)
+    theirs, ours = half_of(1 - y), half_of(y)
+    lh_y = [wire.remote(lh.at[theirs, strip(i)], lh_o.at[:, cols(i, y)], py) for i in range(n)]
+    swap = wire.remote(swap_out, swap_in, py)
+    stores = []
+
+    def start(*copies):
+        for copy in copies:
+            wire.start(copy)
+
+    def arrive(*copies):
+        for copy in copies:
+            copy.wait_recv()
 
     def activate(parity):
         def body(i):
@@ -313,60 +323,6 @@
             act_t[:, rows] = squared(h_all[rows, :]).T
 
         loop(group // block, body)
-
-    for copy in own_h:
-        copy.wait()
-    activate(y)
-
-    downs.wave(1)
-    c_y.wait_recv()
-    wire.start(c_x)
-    wire.start(c_c)
-    for copy in own_up:
-        copy.wait()
-    for copy in up_y:
-        copy.wait_recv()
-    ups.begin()
-    if n > 2:
-        downs.wave(2)
-    c_x.wait_recv()
-    wire.start(c_xc)
-    for copy in h_y:
-        copy.wait_recv()
-    activate(1 - y)
-    c_c.wait_recv()
-    c_xc.wait_recv()
-    own_c.wait()
-
-    tile = min(256, chunk)
-
-    def gd_body(i):
-        columns = pl.ds(pl.multiple_of(i * tile, tile), tile)
-        gd_part[:, columns] = dot(act_t[...], c_all[:, columns]).astype(BF16)
-
-    loop(width // tile, gd_body)
-    gds.seeds(range(n - 2, 0, -1))
-
-    for r in range(3, n):
-        downs.wave(r)
-    own_down.wait()
-
-    slope_rows = min(256, 2 * group)
-
-    def pg_body(i):
-        rows = pl.ds(pl.multiple_of(i * slope_rows, slope_rows), slope_rows)
-        lifted = jnp.maximum(h_all[rows, :].astype(F32), 0.0)
-        pg[rows, :] = (2.0 * dot(c_all[rows, :], down_full[...], 1, 1) * lifted).astype(BF16)
-
-    loop(2 * group // slope_rows, pg_body)
-
-    e_y.wait_recv()
-    wire.start(e_x)
-    wire.start(e_c)
-
-    def store_part(k, parity, value):
-        for q in range(4):
-            part[k, q % 2, q // 2, parity] = value[q * block : (q + 1) * block].astype(BF16)
 
     def column_block(k):
         where = 0
@@ -375,6 +331,32 @@
             where = where + jnp.where(z == i, order[k], 0)
         return pl.ds(pl.multiple_of(where * chunk, chunk), chunk)
 
+    def store_part(k, parity, value):
+        for q in range(4):
+            part[k, q % 2, q // 2, parity] = value[q * block : (q + 1) * block].astype(BF16)
+
+    def gd_dots():
+        def body(i):
+            columns = pl.ds(pl.multiple_of(i * tile, tile), tile)
+            gd_part[:, columns] = dot(act_t[...], c_all[:, columns]).astype(BF16)
+
+        loop(width // tile, body)
+
+    def pg_dots():
+        def body(i):
+            rows = pl.ds(pl.multiple_of(i * slope_rows, slope_rows), slope_rows)
+            lifted = jnp.maximum(h_all[rows, :].astype(F32), 0.0)
+            pg[rows, :] = (2.0 * dot(c_all[rows, :], down_full[...], 1, 1) * lifted).astype(BF16)
+
+        loop(2 * group // slope_rows, body)
+
+    def gu_dots():
+        def body(i):
+            wide = pl.ds(pl.multiple_of(i * tile, tile), tile)
+            gu_part[wide, :] = dot(e_all[:, wide], pg[...], 0, 0).astype(BF16)
+
+        loop(width // tile, body)
+
     def eg_chunk(k):
         wide = column_block(k)
 
@@ -393,56 +375,7 @@
         loop(2, body)
         outs[k].begin()
 
-    eg_chunk(0)
-    for m in range(n - 3, 0, -1):
-        gds.relay(m)
-    ups.wave(1)
-    egs[0].second()
-    eg_chunk(1)
-    e_x.wait_recv()
-    wire.start(e_xc)
-    e_c.wait_recv()
-    e_xc.wait_recv()
-    own_e.wait()
-
-    def gu_body(i):
-        wide = pl.ds(pl.multiple_of(i * tile, tile), tile)
-        gu_part[wide, :] = dot(e_all[:, wide], pg[...], 0, 0).astype(BF16)
-
-    loop(width // tile, gu_body)
-    gus.seeds(range(n - 2, -1, -1))
-    gds.seeds([0])
-
-    x_y.wait_recv()
-    wire.start(x_x)
-    wire.start(x_c)
-    egs[0].third()
-    egs[1].second()
-    for r in range(2, n - 1):
-        ups.wave(r)
-        eg_chunk(r)
-    if n > 2:
-        gds.relay(0)
-    x_own_x.wait_recv()
-    wire.start(x_own_xc)
-    egs[1].third()
-    for r in range(2, n - 1):
-        egs[r].second()
-    x_x.wait_recv()
-    wire.start(x_xc)
-    for copy in (x_own_c, x_c, x_own_xc, x_xc):
-        copy.wait_recv()
-    own_x.wait()
-    for r in range(2, n - 1):
-        egs[r].third()
-
-    if n > 2:
-        ups.wave(n - 1)
-        eg_chunk(n - 1)
-
-    def lh_body(parity):
-        rows = half_of(parity)
-
+    def lh_dots(parity):
         def body(i):
             at = pl.ds(pl.multiple_of(parity * group + i * slope_rows, slope_rows), slope_rows)
             h = dot(x_all[at, :], up_full[...]).astype(BF16)
@@ -450,51 +383,165 @@
             act_l[at, :] = squared(h)
 
         loop(group // slope_rows, body)
-        return rows
-
-    theirs = lh_body(1 - y)
-    lh_y = [
-        wire.remote(lh.at[theirs, strip(i)], lh_o.at[:, cols(i, y)], py) for i in range(n)
-    ]
-    for copy in lh_y:
-        wire.start(copy)
-    egs[n - 1].second()
-    ours = lh_body(y)
-    lh_mine = [wire.copy(lh.at[ours, strip(i)], lh_o.at[:, cols(i, y)]) for i in range(n)]
-    for k in range(n):
-        out_chunk(k)
-        if k:
-            outs[k - 1].second()
-    outs[n - 1].second()
-    for m in range(n - 3, -1, -1):
-        gus.relay(m)
-    egs[n - 1].third()
-    for k in range(n):
-        outs[k].third()
-
-    gds.final(gd_fin, lambda i: i, hb // 4)
-    gd_done = wire.copy(gd_fin, gd_o)
-    per = up_rows // (chunk // 4)
-    gus.final(gu_fin, lambda i: lax.rem(i + (1 - y) * per, 2 * per), chunk // 4)
-    swap_out[...] = gu_fin[pl.ds(pl.multiple_of((1 - y) * up_rows, up_rows), up_rows), :].astype(BF16)
-    swap = wire.remote(swap_out, swap_in, py)
-    wire.start(swap)
-    for k in range(n):
-        egs[k].last(eg_fin, column_block(k))
-    eg_done = wire.copy(eg_fin, eg_o)
-    for k in range(n):
-        outs[k].last(out_fin, pl.ds(k * chunk, chunk))
-    out_done = wire.copy(out_fin, out_o)
-    swap.wait_recv()
-    for i in range(n):
-        gu_out[:, cols(i, y)] = gu_fin[pl.ds(pl.multiple_of(y * up_rows, up_rows), up_rows), strip(i)]
-        gu_out[:, cols(i, 1 - y)] = swap_in[:, strip(i)].astype(F32)
-    gu_done = wire.copy(gu_out, gu_o)
-    for copy in lh_y:
-        copy.wait_recv()
-    for copy in lh_mine + [gd_done, eg_done, out_done, gu_done]:
-        copy.wait()
-    wire.drain()
+
+    def first_sends():
+        downs.begin()
+        start(*c_y, *up_y, *h_y, *e_y, *x_y, x_own_x, x_own_c)
+
+    def ups_begin():
+        for copy in own_up:
+            copy.wait()
+        arrive(*up_y)
+        ups.begin(z < 2, z > n - 3)
+
+    def own_act():
+        for copy in own_h:
+            copy.wait()
+        activate(y)
+
+    def all_c():
+        arrive(*c_c, *c_xc)
+        own_c.wait()
+
+    def all_e():
+        arrive(*e_c, *e_xc)
+        own_e.wait()
+
+    def all_x():
+        arrive(x_own_c, x_own_xc, *x_c, *x_xc)
+        own_x.wait()
+
+    def pass_on(came, *onward):
+        arrive(came)
+        start(*onward)
+
+    def lh_send():
+        start(*lh_y)
+
+    def lh_store():
+        stores.extend(wire.copy(lh.at[ours, strip(i)], lh_o.at[:, cols(i, y)]) for i in range(n))
+
+    def gd_final():
+        gds.final(gd_fin, lambda i: i, hb // 4)
+        stores.append(wire.copy(gd_fin, gd_o))
+
+    def gu_final():
+        per = up_rows // (chunk // 4)
+        gus.final(gu_fin, lambda i: lax.rem(i + (1 - y) * per, 2 * per), chunk // 4)
+        away = pl.ds(pl.multiple_of((1 - y) * up_rows, up_rows), up_rows)
+        swap_out[...] = gu_fin[away, :].astype(BF16)
+        start(swap)
+
+    def gu_store():
+        home = pl.ds(pl.multiple_of(y * up_rows, up_rows), up_rows)
+        arrive(swap)
+        for i in range(n):
+            gu_out[:, cols(i, y)] = gu_fin[home, strip(i)]
+            gu_out[:, cols(i, 1 - y)] = swap_in[:, strip(i)].astype(F32)
+        stores.append(wire.copy(gu_out, gu_o))
+
+    def eg_store():
+        for k in range(n):
+            egs[k].last(eg_fin, column_block(k))
+        stores.append(wire.copy(eg_fin, eg_o))
+
+    def out_store():
+        for k in range(n):
+            outs[k].last(out_fin, pl.ds(k * chunk, chunk))
+        stores.append(wire.copy(out_fin, out_o))
+
+    def close():
+        arrive(*lh_y)
+        for copy in stores:
+            copy.wait()
+        wire.drain()
+
+    def do(name, act, *args):
+        with jax.named_scope(name):
+            act(*args)
+
+    last = n - 1
+    do("first", first_sends)
+    do("own_act", own_act)
+    do("c_y0", pass_on, c_y[0], c_x[0], c_c[0])
+    do("down1", downs.forward, 1)
+    do("c_y1", pass_on, c_y[1], c_x[1], c_c[1])
+    do("x_own_x", pass_on, x_own_x, x_own_xc)
+    do("up_y", ups_begin)
+    for i in (0, 1):
+        do("c_x", pass_on, c_x[i], c_xc[i])
+    for r in range(2, last):
+        do("down2", downs.forward, r)
+    ups.begin(z >= 2, z <= n - 3)
+    do("h_y", arrive, *h_y)
+    do("act2", activate, 1 - y)
+    do("c_all", all_c)
+    do("gd_dots", gd_dots)
+    do("gd_seed", gds.seeds, range(n - 2, 0, -1))
+    do("e_y0", pass_on, e_y[0], e_x[0], e_c[0])
+    do("ups1", ups.forward, 1)
+    for r in range(1, n):
+        do("down_end", downs.ends, r)
+    own_down.wait()
+    do("pg", pg_dots)
+    do("e_y1", pass_on, e_y[1], e_x[1], e_c[1])
+    do("eg0", eg_chunk, 0)
+    do("e_x0", pass_on, e_x[0], e_xc[0])
+    do("eg0_b", egs[0].second)
+    for m in range(n - 3, 0, -1):
+        do("gd_relay", gds.relay, m)
+    do("x_y0", pass_on, x_y[0], x_x[0], x_c[0])
+    do("e_x1", pass_on, e_x[1], e_xc[1])
+    do("e_all", all_e)
+    do("gu_dots", gu_dots)
+    do("gu_seed", gus.seeds, range(n - 2, -1, -1))
+    gds.seeds([0])
+    do("x_y1", pass_on, x_y[1], x_x[1], x_c[1])
+    do("up1_end", ups.ends, 1)
+    do("eg1", eg_chunk, 1)
+    for r in range(2, last):
+        do("ups2", ups.forward, r)
+    do("eg1_b", egs[1].second)
+    do("eg0_c", egs[0].third)
+    do("gd_relay0", gds.relay, 0)
+    for r in range(2, last):
+        do("up2_end", ups.ends, r)
+        do("eg2", eg_chunk, r)
+    do("eg1_c", egs[1].third)
+    for r in range(2, last):
+        do("eg2_b", egs[r].second)
+    for i in (0, 1):
+        do("x_x", pass_on, x_x[i], x_xc[i])
+    do("x_all", all_x)
+    do("up3_end", ups.ends, last)
+    do("lh1", lh_dots, 1 - y)
+    do("lh2", lh_dots, y)
+    lh_store()
+    do("out0", out_chunk, 0)
+    do("eg3", eg_chunk, last)
+    for r in range(2, last):
+        do("eg2_c", egs[r].third)
+    do("out1", out_chunk, 1)
+    do("out0_b", outs[0].second)
+    do("eg3_b", egs[last].second)
+    do("lh_send", lh_send)
+    for m in range(n - 3, 0, -1):
+        do("gu_relay", gus.relay, m)
+    for k in range(2, n):
+        do("out", out_chunk, k)
+        do("out_b", outs[k - 1].second)
+    do("out_b", outs[last].second)
+    do("out0_c", outs[0].third)
+    do("gu_relay0", gus.relay, 0)
+    do("eg3_c", egs[last].third)
+    for k in range(1, n):
+        do("out_c", outs[k].third)
+    do("gu_fin", gu_final)
+    do("eg_fin", eg_store)
+    do("gd_fin", gd_final)
+    do("out_fin", out_store)
+    do("gu_sto", gu_store)
+    do("close", close)
 
 
 def fused(n, later_in, earlier_in, hidden, cot, up, down):
@@ -525,7 +572,7 @@
         vm((block, width), BF16), vm((block, width), BF16),
         vm((hb, width), F32), vm((chunk, half), F32), vm(up.shape, F32),
     ]
-    remote_copies = 8 * (n - 1) + 15 + 3 * n + 6 * n + 1
+    remote_copies = 24 * n + 40
     local_copies = 3 * n + 8
     return pl.pallas_call(
         functools.partial(layer, n),

time: 153 us -> 132 us (0.86)
  Pallas kernels: 145 us -> 125 us
    pallas_call x1, Pallas kernels: 145 us -> 125 us  [fused(): pl.pallas_call(functools.partial(layer, n), out_shape=shapes, in_specs=[a...]
where the time goes in v1:
time: 132 us
  Pallas kernels  125 us (95%)
  other arithmetic  3.96 us (3%)
  local copies, waits for them, and re-layouts  2.58 us (2%)
    pallas_call x1, Pallas kernels, fused(): pl.pallas_call(functools.partial(layer, n), out_shape=shapes, in_specs=[a...  125 us
    add x2, other arithmetic, shards(): return (out, later_hidden, eg, up_sum + scale * gu, down_sum + scale * gd)  3.96 us

profile of v1, /device:TPU:0, one launch (start us, length us, event | category | flops | bytes accessed | tf_op | source)
XLA Modules:
  0.0 132.1 jit_solution(16148264138695201571)
XLA Ops:
  0.6 124.8 %layer.1 = (bf16[128,2048]{1,0:T(8,128)(2,1)}, bf16[512,1024]{1,0:T(8,128)(2,1)}, bf16[128,2048]{1,0:T(8,128)(2,1)}, f32[256,1024]{1,0:T(8,128)}, f32[128,2048]{1,0:T(8,128)}) custom-call(bf16[128,2048]{1,0:T(8,128)(2,1)} %later_in.1, bf16[512,2048]{1,0:T(8,128)(2,1)} %earlier_in.1, bf16[512,1024]{1,0:T(8,128)(2,1)} %hidden.1, bf16[512,2048]{1,0:T(8,128)(2,1)} %cot.1, ...), custom_call_target="tpu_custom_call" | custom-call | tf_op jit(solution)/shard_map/layer/pallas_call | solution.py:577
  125.5 0.0 copy-start
  125.5 0.0 copy-start.1
  125.5 2.9 %multiply_add_fusion.1 = f32[256,1024]{1,0:T(8,128)} fusion(f32[256,1024]{1,0:T(8,128)} %param.14, f32[256,1024]{1,0:T(8,128)} %get-tuple-element.13), kind=kLoop, calls=%fused_computation.1 | loop fusion | flops 524288 | bytes 3145728 | tf_op jit(solution)/shard_map/add | solution.py:626
  128.4 0.0 copy-done
  128.4 0.0 copy-done.1
  128.4 0.0 copy-start.4
  128.4 0.0 copy-start.2
  128.4 1.1 multiply_add_fusion
  129.5 0.0 copy-done.4
  129.5 0.0 copy-start.3
  129.5 0.8 copy.16
  130.3 0.0 copy-done.2
  130.3 1.0 copy.17
  131.3 0.0 copy-done.3
  131.3 0.8 copy.18
Async XLA Ops:
  125.5 2.9 %copy-start = (f32[128,2048]{1,0:T(8,128)S(1)}, f32[128,2048]{1,0:T(8,128)}, u32[]{:S(2)}) copy-start(f32[128,2048]{1,0:T(8,128)} %param.15) | copy-start | bytes 3145732
  125.5 2.9 %copy-start.1 = (f32[128,2048]{1,0:T(8,128)S(1)}, f32[128,2048]{1,0:T(8,128)}, u32[]{:S(2)}) copy-start(f32[128,2048]{1,0:T(8,128)} %get-tuple-element.14) | copy-start | bytes 3145732
  128.4 1.1 copy-start.4
  128.4 1.9 %copy-start.2 = (bf16[512,1024]{1,0:T(8,128)(2,1)S(1)}, bf16[512,1024]{1,0:T(8,128)(2,1)}, u32[]{:S(2)}) copy-start(bf16[512,1024]{1,0:T(8,128)(2,1)} %get-tuple-element.21) | copy-start | bytes 3145732
  129.5 1.8 %copy-start.3 = (bf16[128,2048]{1,0:T(8,128)(2,1)S(1)}, bf16[128,2048]{1,0:T(8,128)(2,1)}, u32[]{:S(2)}) copy-start(bf16[128,2048]{1,0:T(8,128)(2,1)} %get-tuple-element.22) | copy-start | bytes 1572868

commit v2 on v1

--- a/solution.py
+++ b/solution.py
@@ -74,64 +74,84 @@
 
 
 class Line:
-    def __init__(self, wire, full, rows, own, z, n, left, right):
+    def __init__(self, wire, full, rows, own, swap, z, n, left, right):
         self.wire, self.z, self.n = wire, z, n
         self.right, self.left = {}, {}
-
-        def block(i):
-            return full.at[pl.ds(pl.multiple_of(lax.rem(i + n, n) * rows, rows), rows)]
-
-        for r in range(1, n):
-            src = own if r == 1 else block(z - r + 1)
-            self.right[r] = wire.remote(src, block(z - r + 1), right)
-            src = own if r == 1 else block(z + r - 1)
-            self.left[r] = wire.remote(src, block(z + r - 1), left)
-
-    def begin(self, right=True, left=True):
-        self.wire.start(self.right[1], both(self.z < self.n - 1, right))
-        self.wire.start(self.left[1], both(self.z > 0, left))
-
-    def forward(self, r):
+        size = rows // 2
+
+        def half(i, p):
+            base = lax.rem(i + n, n) * rows + lax.rem(swap + p, 2) * size
+            return full.at[pl.ds(pl.multiple_of(base, size), size)]
+
+        for p in (0, 1):
+            first = half(z, p)
+            if own is not None:
+                first = own.at[pl.ds(pl.multiple_of(lax.rem(swap + p, 2) * size, size), size)]
+            for r in range(1, n):
+                src = first if r == 1 else half(z - r + 1, p)
+                self.right[r, p] = wire.remote(src, half(z - r + 1, p), right)
+                src = first if r == 1 else half(z + r - 1, p)
+                self.left[r, p] = wire.remote(src, half(z + r - 1, p), left)
+
+    def begin(self, p, right=True, left=True):
+        self.wire.start(self.right[1, p], both(self.z < self.n - 1, right))
+        self.wire.start(self.left[1, p], both(self.z > 0, left))
+
+    def begin_at(self, stage, p):
+        self.begin(p, self.z == stage, self.z == self.n - 1 - stage)
+
+    def forward(self, r, p, outer=None):
         z, n = self.z, self.n
         rightward, leftward = both(z >= r, z < n - 1), both(z <= n - 1 - r, z > 0)
-        pl.when(rightward)(self.right[r].wait_recv)
-        self.wire.start(self.right[r + 1], rightward)
-        pl.when(leftward)(self.left[r].wait_recv)
-        self.wire.start(self.left[r + 1], leftward)
+        if outer is not None:
+            rightward = both(rightward, (z == r) == outer)
+            leftward = both(leftward, (z == n - 1 - r) == outer)
+        pl.when(rightward)(self.right[r, p].wait_recv)
+        self.wire.start(self.right[r + 1, p], rightward)
+        pl.when(leftward)(self.left[r, p].wait_recv)
+        self.wire.start(self.left[r + 1, p], leftward)
 
     def ends(self, r):
         z, n = self.z, self.n
-        pl.when(both(z >= r, z == n - 1))(self.right[r].wait_recv)
-        pl.when(both(z <= n - 1 - r, z == 0))(self.left[r].wait_recv)
+        for p in (0, 1):
+            pl.when(both(z >= r, z == n - 1))(self.right[r, p].wait_recv)
+            pl.when(both(z <= n - 1 - r, z == 0))(self.left[r, p].wait_recv)
 
 
 class Sums:
-    def __init__(self, wire, part, inbox, relayed, rows, z, n, left, right):
+    def __init__(self, wire, part, inbox, relayed, rows, swap, z, n, left, right):
         self.wire, self.part, self.inbox, self.relayed = wire, part, inbox, relayed
-        self.rows, self.z, self.n = rows, z, n
+        self.rows, self.size, self.swap, self.z, self.n = rows, rows // 2, swap, z, n
         self.seed, self.pass_on = {}, {}
         for way, device in ((0, right), (1, left)):
             for m in range(n - 1):
-                slot = wire.slot()
-                dst = inbox.at[way, m]
-                self.seed[way, m] = wire.remote(part.at[self.span(way, m)], dst, device, slot)
-                if m < n - 2:
-                    self.pass_on[way, m] = wire.remote(relayed.at[way, m], dst, device, slot)
-
-    def span(self, way, m, lo=0, size=None):
+                for p in (0, 1):
+                    slot = wire.slot()
+                    at = pl.ds(p * self.size, self.size)
+                    dst = inbox.at[way, m, at]
+                    src = part.at[self.span(way, m, p)]
+                    self.seed[way, m, p] = wire.remote(src, dst, device, slot)
+                    if m < n - 2:
+                        src = relayed.at[way, m, at]
+                        self.pass_on[way, m, p] = wire.remote(src, dst, device, slot)
+
+    def half(self, p):
+        return lax.rem(self.swap + p, 2) * self.size
+
+    def span(self, way, m, p):
         ahead = self.z + 1 + m if way == 0 else self.z - 1 - m
-        base = lax.rem(ahead + 2 * self.n, self.n) * self.rows
-        size = self.rows if size is None else size
-        return pl.ds(pl.multiple_of(base + lo, size), size)
+        base = lax.rem(ahead + 2 * self.n, self.n) * self.rows + self.half(p)
+        return pl.ds(pl.multiple_of(base, self.size), self.size)
 
     def seeds(self, ms):
         for m in ms:
-            self.wire.start(self.seed[0, m], self.z == 0)
-            self.wire.start(self.seed[1, m], self.z == self.n - 1)
-
-    def relay(self, m):
+            for p in (0, 1):
+                self.wire.start(self.seed[0, m, p], self.z == 0)
+                self.wire.start(self.seed[1, m, p], self.z == self.n - 1)
+
+    def relay(self, m, p):
         z, n = self.z, self.n
-        tile = self.rows // 4
+        at = pl.ds(p * self.size, self.size)
         for way in (0, 1):
             if way == 0:
                 when = both(z >= 1, z + 1 + m <= n - 1)
@@ -139,35 +159,24 @@
                 when = both(z <= n - 2, z - 1 - m >= 0)
 
             def add(way=way):
-                self.seed[way, m + 1].wait_recv()
-
-                def body(i):
-                    lo = pl.multiple_of(i * tile, tile)
-                    mine = self.part[self.span(way, m, lo, tile), :].astype(F32)
-                    came = self.inbox[way, m + 1, pl.ds(lo, tile), :].astype(F32)
-                    self.relayed[way, m, pl.ds(lo, tile), :] = (mine + came).astype(BF16)
-
-                loop(4, body)
+                self.seed[way, m + 1, p].wait_recv()
+                mine = self.part[self.span(way, m, p), :].astype(F32)
+                came = self.inbox[way, m + 1, at, :].astype(F32)
+                self.relayed[way, m, at, :] = (mine + came).astype(BF16)
 
             pl.when(when)(add)
-            self.wire.start(self.pass_on[way, m], when)
-
-    def final(self, out, order, tile):
+            self.wire.start(self.pass_on[way, m, p], when)
+
+    def total(self, p):
         z, n = self.z, self.n
-        pl.when(z >= 1)(self.seed[0, 0].wait_recv)
-        pl.when(z <= n - 2)(self.seed[1, 0].wait_recv)
-        up, down = (z >= 1).astype(F32), (z <= n - 2).astype(F32)
-        base = z * self.rows
-
-        def body(i):
-            lo = pl.multiple_of(order(i) * tile, tile)
-            rows = pl.ds(lo, tile)
-            mine = self.part[pl.ds(pl.multiple_of(base + lo, tile), tile), :].astype(F32)
-            first = jnp.where(z >= 1, self.inbox[0, 0, rows, :].astype(F32), 0.0)
-            second = jnp.where(z <= n - 2, self.inbox[1, 0, rows, :].astype(F32), 0.0)
-            out[rows, :] = mine + first + second
-
-        loop(self.rows // tile, body)
+        pl.when(z >= 1)(self.seed[0, 0, p].wait_recv)
+        pl.when(z <= n - 2)(self.seed[1, 0, p].wait_recv)
+        at = pl.ds(p * self.size, self.size)
+        base = z * self.rows + self.half(p)
+        mine = self.part[pl.ds(pl.multiple_of(base, self.size), self.size), :].astype(F32)
+        first = jnp.where(z >= 1, self.inbox[0, 0, at, :].astype(F32), 0.0)
+        second = jnp.where(z <= n - 2, self.inbox[1, 0, at, :].astype(F32), 0.0)
+        return mine + first + second
 
 
 class Plane:
@@ -207,13 +216,14 @@
 
 
 def layer(
-    n, later_in, earlier_in, hidden, cot, up, down,
+    n, later_in, earlier_in, hidden, cot, up, down, up_sum, down_sum,
     out_o, lh_o, eg_o, gu_o, gd_o,
     c_all, e_all, x_all, h_all, act_t, pg, up_full, down_full, gd_part, gu_part,
-    gd_in, gd_relay, gu_in, gu_relay, swap_out, swap_in, lh, act_l,
-    part, in_a, to_b, in_b, to_c, in_c, eg_fin, out_fin, gd_fin, gu_fin, gu_out,
-    send, recv, local,
+    gd_in, gd_relay, gu_in, gu_relay, swap_out, swap_in, lh, act_l, lh_sum,
+    *rest,
 ):
+    eg_bufs, out_bufs = rest[:6], rest[6:12]
+    eg_fin, out_fin, gd_fin, gu_fin, send, recv, local = rest[12:]
     fs, tp = lax.axis_index("fs"), lax.axis_index("tp")
     z, y = fs // 2, fs % 2
     x, c = tp // 2, tp % 2
@@ -257,6 +267,9 @@
     own_down = wire.copy(down, down_full.at[pl.ds(pl.multiple_of(z * hb, hb), hb)])
     own_e = wire.copy(earlier_in, e_all.at[half_of(y)])
     own_x = wire.copy(later_in, x_all.at[rows_of(y, tp)])
+    own_up_sum = wire.copy(up_sum, gu_fin)
+    own_down_sum = wire.copy(down_sum, gd_fin)
+    scale = float(group * 2 * n) ** (-0.5)
 
     pl.semaphore_wait(barrier, 3 + (z > 0).astype(jnp.int32) + (z < n - 1).astype(jnp.int32))
 
@@ -278,9 +291,8 @@
             ))
         return zip(*made)
 
-    downs = Line(wire, down_full, hb, down, z, n, left, right)
-    up_block = up_full.at[pl.ds(pl.multiple_of(z * chunk, chunk), chunk)]
-    ups = Line(wire, up_full, chunk, up_block, z, n, left, right)
+    downs = Line(wire, down_full, hb, down, y, z, n, left, right)
+    ups = Line(wire, up_full, chunk, None, y, z, n, left, right)
     c_y, c_x, c_c, c_xc = spread(c_all, cot, tp * block, 2)
     e_y, e_x, e_c, e_xc = spread(e_all, earlier_in, tp * block, 2)
     x_y, x_x, x_c, x_xc = spread(x_all, later_in, 0, 2)
@@ -297,11 +309,11 @@
         for i in range(n)
     ]
 
-    gds = Sums(wire, gd_part, gd_in, gd_relay, hb, z, n, left, right)
-    gus = Sums(wire, gu_part, gu_in, gu_relay, chunk, z, n, left, right)
-    bufs = (part, in_a, to_b, in_b, to_c, in_c)
-    planes = [Plane(wire, bufs, k, (x, y, c), (px, py, pc), k >= n) for k in range(2 * n)]
-    egs, outs = planes[:n], planes[n:]
+    gds = Sums(wire, gd_part, gd_in, gd_relay, hb, 1 - y, z, n, left, right)
+    gus = Sums(wire, gu_part, gu_in, gu_relay, chunk, 1 - y, z, n, left, right)
+    at, peers = (x, y, c), (px, py, pc)
+    egs = [Plane(wire, eg_bufs, k, at, peers, k >= n - 1) for k in range(n)]
+    outs = [Plane(wire, out_bufs, k, at, peers, True) for k in range(2 * n)]
     tile = min(256, chunk)
     slope_rows = min(256, 2 * group)
     theirs, ours = half_of(1 - y), half_of(y)
@@ -331,14 +343,18 @@
             where = where + jnp.where(z == i, order[k], 0)
         return pl.ds(pl.multiple_of(where * chunk, chunk), chunk)
 
-    def store_part(k, parity, value):
+    def store_part(plane, parity, value):
         for q in range(4):
-            part[k, q % 2, q // 2, parity] = value[q * block : (q + 1) * block].astype(BF16)
-
-    def gd_dots():
+            plane.part[q % 2, q // 2, parity] = value[q * block : (q + 1) * block].astype(BF16)
+
+    far = jnp.where(z < n // 2, n - 1, 0)
+
+    def gd_dots(row, size):
+        rows = pl.ds(pl.multiple_of(row, hb), size)
+
         def body(i):
             columns = pl.ds(pl.multiple_of(i * tile, tile), tile)
-            gd_part[:, columns] = dot(act_t[...], c_all[:, columns]).astype(BF16)
+            gd_part[rows, columns] = dot(act_t[rows, :], c_all[:, columns]).astype(BF16)
 
         loop(width // tile, body)
 
@@ -361,38 +377,57 @@
         wide = column_block(k)
 
         def body(parity):
-            store_part(k, parity, dot(pg[half_of(parity), :], up_full[wide, :], 1, 1))
+            store_part(egs[k], parity, dot(pg[half_of(parity), :], up_full[wide, :], 1, 1))
 
         loop(2, body)
         egs[k].begin()
 
+    def out_columns(k):
+        return pl.ds(k * (chunk // 2), chunk // 2)
+
     def out_chunk(k):
-        wide = pl.ds(k * chunk, chunk)
+        wide = out_columns(k)
 
         def body(parity):
-            store_part(n + k, parity, dot(act_l[half_of(parity), :], down_full[:, wide]))
+            store_part(outs[k], parity, dot(act_l[half_of(parity), :], down_full[:, wide]))
 
         loop(2, body)
         outs[k].begin()
 
-    def lh_dots(parity):
+    def lh_early():
+        blocks = [column_block(k) for k in range(n - 1)]
+
+        def body(i):
+            at = pl.ds(pl.multiple_of(i * slope_rows, slope_rows), slope_rows)
+            total = dot(x_all[at, blocks[0]], up_full[blocks[0], :])
+            for wide in blocks[1:]:
+                total = total + dot(x_all[at, wide], up_full[wide, :])
+            lh_sum[at, :] = total
+
+        loop(2 * group // slope_rows, body)
+
+    def lh_late(parity):
+        wide = column_block(n - 1)
+
         def body(i):
             at = pl.ds(pl.multiple_of(parity * group + i * slope_rows, slope_rows), slope_rows)
-            h = dot(x_all[at, :], up_full[...]).astype(BF16)
+            h = (lh_sum[at, :] + dot(x_all[at, wide], up_full[wide, :])).astype(BF16)
             lh[at, :] = h
             act_l[at, :] = squared(h)
 
         loop(group // slope_rows, body)
 
     def first_sends():
-        downs.begin()
+        for p in (0, 1):
+            downs.begin(p)
         start(*c_y, *up_y, *h_y, *e_y, *x_y, x_own_x, x_own_c)
-
-    def ups_begin():
         for copy in own_up:
             copy.wait()
-        arrive(*up_y)
-        ups.begin(z < 2, z > n - 3)
+        ups.begin_at(0, 0)
+
+    def relay(sums, m):
+        for p in (0, 1):
+            sums.relay(m, p)
 
     def own_act():
         for copy in own_h:
@@ -422,32 +457,39 @@
         stores.extend(wire.copy(lh.at[ours, strip(i)], lh_o.at[:, cols(i, y)]) for i in range(n))
 
     def gd_final():
-        gds.final(gd_fin, lambda i: i, hb // 4)
+        own_down_sum.wait()
+        for p in (0, 1):
+            rows = pl.ds(pl.multiple_of(gds.half(p), hb // 2), hb // 2)
+            gd_fin[rows, :] = gd_fin[rows, :] + scale * gds.total(p)
         stores.append(wire.copy(gd_fin, gd_o))
 
-    def gu_final():
-        per = up_rows // (chunk // 4)
-        gus.final(gu_fin, lambda i: lax.rem(i + (1 - y) * per, 2 * per), chunk // 4)
-        away = pl.ds(pl.multiple_of((1 - y) * up_rows, up_rows), up_rows)
-        swap_out[...] = gu_fin[away, :].astype(BF16)
+    def gu_away():
+        swap_out[...] = gus.total(0).astype(BF16)
         start(swap)
 
+    def gu_home():
+        own_up_sum.wait()
+        total = gus.total(1)
+        for i in range(n):
+            kept = total[:, i * hb : (i + 1) * hb]
+            gu_fin[:, cols(i, y)] = gu_fin[:, cols(i, y)] + scale * kept
+
     def gu_store():
-        home = pl.ds(pl.multiple_of(y * up_rows, up_rows), up_rows)
         arrive(swap)
         for i in range(n):
-            gu_out[:, cols(i, y)] = gu_fin[home, strip(i)]
-            gu_out[:, cols(i, 1 - y)] = swap_in[:, strip(i)].astype(F32)
-        stores.append(wire.copy(gu_out, gu_o))
+            came = swap_in[:, strip(i)].astype(F32)
+            gu_fin[:, cols(i, 1 - y)] = gu_fin[:, cols(i, 1 - y)] + scale * came
+        stores.append(wire.copy(gu_fin, gu_o))
 
     def eg_store():
         for k in range(n):
             egs[k].last(eg_fin, column_block(k))
         stores.append(wire.copy(eg_fin, eg_o))
 
+    def out_last(k):
+        outs[k].last(out_fin, out_columns(k))
+
     def out_store():
-        for k in range(n):
-            outs[k].last(out_fin, pl.ds(k * chunk, chunk))
         stores.append(wire.copy(out_fin, out_o))
 
     def close():
@@ -464,22 +506,34 @@
     do("first", first_sends)
     do("own_act", own_act)
     do("c_y0", pass_on, c_y[0], c_x[0], c_c[0])
-    do("down1", downs.forward, 1)
+    do("down10", downs.forward, 1, 0)
     do("c_y1", pass_on, c_y[1], c_x[1], c_c[1])
+    do("down11", downs.forward, 1, 1)
+    ups.begin_at(1, 0)
     do("x_own_x", pass_on, x_own_x, x_own_xc)
-    do("up_y", ups_begin)
+    do("up_y", arrive, *up_y)
+    for stage in (0, 1):
+        ups.begin_at(stage, 1)
+    for r in range(2, last):
+        do("down20", downs.forward, r, 0)
     for i in (0, 1):
         do("c_x", pass_on, c_x[i], c_xc[i])
     for r in range(2, last):
-        do("down2", downs.forward, r)
-    ups.begin(z >= 2, z <= n - 3)
+        do("down21", downs.forward, r, 1)
+        for p in (0, 1):
+            ups.begin_at(r, p)
     do("h_y", arrive, *h_y)
     do("act2", activate, 1 - y)
+    for p in (0, 1):
+        do("ups1e", ups.forward, 1, p, True)
     do("c_all", all_c)
-    do("gd_dots", gd_dots)
-    do("gd_seed", gds.seeds, range(n - 2, 0, -1))
+    do("gd_far", gd_dots, far * hb, hb)
+    gds.seeds([n - 2])
+    do("gd_dots", gd_dots, jnp.where(far == 0, hb, 0), half - hb)
+    do("gd_seed", gds.seeds, range(n - 3, 0, -1))
     do("e_y0", pass_on, e_y[0], e_x[0], e_c[0])
-    do("ups1", ups.forward, 1)
+    for p in (0, 1):
+        do("ups1", ups.forward, 1, p, False)
     for r in range(1, n):
         do("down_end", downs.ends, r)
     own_down.wait()
@@ -489,7 +543,7 @@
     do("e_x0", pass_on, e_x[0], e_xc[0])
     do("eg0_b", egs[0].second)
     for m in range(n - 3, 0, -1):
-        do("gd_relay", gds.relay, m)
+        do("gd_relay", relay, gds, m)
     do("x_y0", pass_on, x_y[0], x_x[0], x_c[0])
     do("e_x1", pass_on, e_x[1], e_xc[1])
     do("e_all", all_e)
@@ -500,51 +554,58 @@
     do("up1_end", ups.ends, 1)
     do("eg1", eg_chunk, 1)
     for r in range(2, last):
-        do("ups2", ups.forward, r)
+        for p in (0, 1):
+            do("ups2", ups.forward, r, p)
     do("eg1_b", egs[1].second)
     do("eg0_c", egs[0].third)
-    do("gd_relay0", gds.relay, 0)
+    do("gd_relay0", relay, gds, 0)
     for r in range(2, last):
         do("up2_end", ups.ends, r)
         do("eg2", eg_chunk, r)
-    do("eg1_c", egs[1].third)
     for r in range(2, last):
         do("eg2_b", egs[r].second)
+    do("eg1_c", egs[1].third)
     for i in (0, 1):
         do("x_x", pass_on, x_x[i], x_xc[i])
     do("x_all", all_x)
+    do("lh_early", lh_early)
+    for r in range(2, last):
+        do("eg2_c", egs[r].third)
     do("up3_end", ups.ends, last)
-    do("lh1", lh_dots, 1 - y)
-    do("lh2", lh_dots, y)
+    do("eg3", eg_chunk, last)
+    do("lh_late1", lh_late, 1 - y)
+    do("lh_send", lh_send)
+    do("lh_late2", lh_late, y)
+    do("eg3_b", egs[last].second)
     lh_store()
     do("out0", out_chunk, 0)
-    do("eg3", eg_chunk, last)
-    for r in range(2, last):
-        do("eg2_c", egs[r].third)
-    do("out1", out_chunk, 1)
-    do("out0_b", outs[0].second)
-    do("eg3_b", egs[last].second)
-    do("lh_send", lh_send)
     for m in range(n - 3, 0, -1):
-        do("gu_relay", gus.relay, m)
-    for k in range(2, n):
+        do("gu_relay", relay, gus, m)
+    pieces = 2 * n
+    for k in range(1, pieces):
         do("out", out_chunk, k)
         do("out_b", outs[k - 1].second)
-    do("out_b", outs[last].second)
-    do("out0_c", outs[0].third)
-    do("gu_relay0", gus.relay, 0)
+    do("out_b", outs[pieces - 1].second)
     do("eg3_c", egs[last].third)
+    do("out_c", outs[0].third)
+    do("gu_relay0", relay, gus, 0)
     for k in range(1, n):
         do("out_c", outs[k].third)
-    do("gu_fin", gu_final)
+    do("gu_away", gu_away)
     do("eg_fin", eg_store)
+    do("gu_home", gu_home)
+    for k in range(n, pieces):
+        do("out_c", outs[k].third)
+        do("out_last", out_last, k - n)
+    do("gu_sto", gu_store)
     do("gd_fin", gd_final)
+    for k in range(pieces - n, pieces):
+        do("out_last", out_last, k)
     do("out_fin", out_store)
-    do("gu_sto", gu_store)
     do("close", close)
 
 
-def fused(n, later_in, earlier_in, hidden, cot, up, down):
+def fused(n, later_in, earlier_in, hidden, cot, up, down, up_sum, down_sum):
     group, width = earlier_in.shape
     block, hb, up_rows = later_in.shape[0], down.shape[0], up.shape[0]
     half, tokens, chunk = n * hb, 2 * group, 2 * up_rows
@@ -557,6 +618,11 @@
         jax.ShapeDtypeStruct(down.shape, F32),
     )
     vm = pltpu.VMEM
+
+    def plane(count, columns):
+        leading = (2, 2, 2), (2, 2), (2,), (2,), (), ()
+        return [vm((count, *lead, block, columns), BF16) for lead in leading]
+
     scratch = [
         vm((tokens, width), BF16), vm((tokens, width), BF16), vm((tokens, width), BF16),
         vm((tokens, half), BF16), vm((half, tokens), BF16), vm((tokens, half), BF16),
@@ -565,19 +631,17 @@
         vm((2, n - 1, hb, width), BF16), vm((2, max(n - 2, 1), hb, width), BF16),
         vm((2, n - 1, chunk, half), BF16), vm((2, max(n - 2, 1), chunk, half), BF16),
         vm((up_rows, half), BF16), vm((up_rows, half), BF16),
-        vm((tokens, half), BF16), vm((tokens, half), BF16),
-        vm((2 * n, 2, 2, 2, block, chunk), BF16), vm((2 * n, 2, 2, block, chunk), BF16),
-        vm((2 * n, 2, block, chunk), BF16), vm((2 * n, 2, block, chunk), BF16),
-        vm((2 * n, block, chunk), BF16), vm((2 * n, block, chunk), BF16),
+        vm((tokens, half), BF16), vm((tokens, half), BF16), vm((tokens, half), F32),
+        *plane(n, chunk), *plane(2 * n, chunk // 2),
         vm((block, width), BF16), vm((block, width), BF16),
-        vm((hb, width), F32), vm((chunk, half), F32), vm(up.shape, F32),
+        vm((hb, width), F32), vm(up.shape, F32),
     ]
-    remote_copies = 24 * n + 40
-    local_copies = 3 * n + 8
+    remote_copies = 36 * n + 40
+    local_copies = 3 * n + 10
     return pl.pallas_call(
         functools.partial(layer, n),
         out_shape=shapes,
-        in_specs=[any_space] * 6,
+        in_specs=[any_space] * 8,
         out_specs=(any_space,) * 5,
         scratch_shapes=scratch + [
             pltpu.SemaphoreType.DMA((remote_copies,)),
@@ -588,10 +652,44 @@
             collective_id=0, has_side_effects=True, vmem_limit_bytes=VMEM_BYTES
         ),
         name="layer",
-    )(later_in, earlier_in, hidden, cot, up, down)
-
-
-def portable(later_in, earlier_in, hidden, cot, up, down):
+    )(later_in, earlier_in, hidden, cot, up, down, up_sum, down_sum)
+
+
+def hand_on(*refs):
+    count = (len(refs) - 2) // 3
+    came, gone = refs[-2:]
+    sources, results, held = refs[:count], refs[count : 2 * count], refs[2 * count : 3 * count]
+    pieces = []
+    for source, result, hold in zip(sources, results, held):
+        parts = 2 if source.dtype == F32 or source.shape[0] > LANES * 2 else 1
+        size = source.shape[0] // parts
+        for p in range(parts):
+            at, i = pl.ds(p * size, size), len(pieces)
+            read = pltpu.make_async_copy(source.at[at], hold.at[at], came.at[i])
+            write = pltpu.make_async_copy(hold.at[at], result.at[at], gone.at[i])
+            read.start()
+            pieces.append((read, write))
+    for read, write in pieces:
+        read.wait()
+        write.start()
+    for _, write in pieces:
+        write.wait()
+
+
+def handed_on(arrays):
+    any_space = pl.BlockSpec(memory_space=pl.ANY)
+    return pl.pallas_call(
+        hand_on,
+        out_shape=tuple(jax.ShapeDtypeStruct(a.shape, a.dtype) for a in arrays),
+        in_specs=[any_space] * len(arrays),
+        out_specs=(any_space,) * len(arrays),
+        scratch_shapes=[pltpu.VMEM(a.shape, a.dtype) for a in arrays]
+        + [pltpu.SemaphoreType.DMA((2 * len(arrays),))] * 2,
+        name="hand_on",
+    )(*arrays)
+
+
+def portable(n_fs, later_in, earlier_in, hidden, cot, up, down, up_sum, down_sum):
     def split_sum(partial, axis):
         return lax.psum_scatter(partial.astype(F32), axis, scatter_dimension=0, tiled=True)
 
@@ -605,25 +703,22 @@
     eg = split_sum(dot(pre, up_full, 1, 1).astype(BF16), "tp").astype(BF16)
     later_hidden = dot(rows, up_full).astype(BF16)
     out = split_sum(dot(squared(later_hidden), down_full).astype(BF16), "tp").astype(BF16)
-    return out, later_hidden, eg, gu, gd
+    scale = float(earlier_in.shape[0] * n_fs) ** (-0.5)
+    return out, later_hidden, eg, up_sum + scale * gu, down_sum + scale * gd
 
 
 def solution(mesh):
     n_fs, n_tp = mesh.shape["fs"], mesh.shape["tp"]
 
-    def shards(
-        later_input, earlier_input, earlier_hidden, cotangent, up_weight, down_weight, up_sum, down_sum
-    ):
-        scale = float(earlier_input.shape[0] * n_fs) ** (-0.5)
-        args = (later_input, earlier_input, earlier_hidden, cotangent, up_weight, down_weight)
+    def shards(*args):
+        later_input, up_weight, down_weight = args[0], args[4], args[5]
         planes = n_fs // 2
         fits = (
             n_tp == 4 and n_fs % 2 == 0 and 2 < planes <= 4
             and down_weight.shape[0] % LANES == 0 and up_weight.shape[0] % LANES == 0
             and later_input.shape[0] % LANES == 0
         )
-        out, later_hidden, eg, gu, gd = fused(planes, *args) if fits else portable(*args)
-        return out, later_hidden, eg, up_sum + scale * gu, down_sum + scale * gd
+        return handed_on(fused(planes, *args)) if fits else portable(n_fs, *args)
 
     in_specs = (
         P(("fs", "tp"), None), P("fs", None), P("fs", "tp"), P("fs", None),

time: 132 us -> 120 us (0.909)
  Pallas kernels: 125 us -> 119 us
  other arithmetic: 3.96 us -> 0 us
  local copies, waits for them, and re-layouts: 2.58 us -> 0 us
    pallas_call x1, Pallas kernels: 125 us -> 116 us  [fused(): pl.pallas_call(functools.partial(layer, n), out_shape=shapes, in_specs=[a...]
    add x2 -> x0, other arithmetic: 3.96 us -> none  [shards(): return (out, later_hidden, eg, up_sum + scale * gu, down_sum + scale * gd)]
    pallas_call x0 -> x1, Pallas kernels: none -> 3.61 us  [handed_on(): pl.pallas_call(hand_on, out_shape=tuple((jax.ShapeDtypeStruct(a.shape, a....]
    unnamed x13 -> x0, local copies, waits for them, and re-layouts: 2.58 us -> none
where the time goes in v2:
time: 120 us
  Pallas kernels  119 us (99%)
    pallas_call x1, Pallas kernels, fused(): pl.pallas_call(functools.partial(layer, n), out_shape=shapes, in_specs=[a...  116 us
    pallas_call x1, Pallas kernels, handed_on(): pl.pallas_call(hand_on, out_shape=tuple((jax.ShapeDtypeStruct(a.shape, a....  3.61 us

profile of v2, /device:TPU:0, one launch (start us, length us, event | category | flops | bytes accessed | tf_op | source)
XLA Modules:
  0.0 119.8 jit_solution(8114688827453520361)
XLA Ops:
  0.6 115.5 %layer.1 = (bf16[128,2048]{1,0:T(8,128)(2,1)}, bf16[512,1024]{1,0:T(8,128)(2,1)}, bf16[128,2048]{1,0:T(8,128)(2,1)}, f32[256,1024]{1,0:T(8,128)}, f32[128,2048]{1,0:T(8,128)}) custom-call(bf16[128,2048]{1,0:T(8,128)(2,1)} %later_in.1, bf16[512,2048]{1,0:T(8,128)(2,1)} %earlier_in.1, bf16[512,1024]{1,0:T(8,128)(2,1)} %hidden.1, bf16[512,2048]{1,0:T(8,128)(2,1)} %cot.1, ...), custom_call_target="tpu_custom_call" | custom-call | tf_op jit(solution)/shard_map/layer/pallas_call | solution.py:641
  116.2 3.6 %hand_on.1 = (bf16[128,2048]{1,0:T(8,128)(2,1)}, bf16[512,1024]{1,0:T(8,128)(2,1)}, bf16[128,2048]{1,0:T(8,128)(2,1)}, f32[256,1024]{1,0:T(8,128)}, f32[128,2048]{1,0:T(8,128)}) custom-call(bf16[128,2048]{1,0:T(8,128)(2,1)} %get-tuple-element.10.refs_0_, bf16[512,1024]{1,0:T(8,128)(2,1)} %get-tuple-element.11.refs_1_, ...), custom_call_target="tpu_custom_call" | custom-call | tf_op jit(solution)/shard_map/hand_on/pallas_call | solution.py:681

commit v3 on v2

--- a/solution.py
+++ b/solution.py
@@ -10,7 +10,7 @@
 F32, BF16 = jnp.float32, jnp.bfloat16
 MESH = pl.DeviceIdType.MESH
 LANES = 128
-VMEM_BYTES = 67_043_328
+VMEM_BYTES = 62_000_000
 
 
 def dot(a, b, ca=1, cb=0):
@@ -111,9 +111,9 @@
         pl.when(leftward)(self.left[r, p].wait_recv)
         self.wire.start(self.left[r + 1, p], leftward)
 
-    def ends(self, r):
+    def ends(self, r, halves=(0, 1)):
         z, n = self.z, self.n
-        for p in (0, 1):
+        for p in halves:
             pl.when(both(z >= r, z == n - 1))(self.right[r, p].wait_recv)
             pl.when(both(z <= n - 1 - r, z == 0))(self.left[r, p].wait_recv)
 
@@ -180,14 +180,18 @@
 
 
 class Plane:
-    def __init__(self, wire, bufs, k, at, peers, x_first):
+    def __init__(self, wire, bufs, k, at, peers, x_first, slots=None):
         self.part, self.in_a, self.to_b, self.in_b, self.to_c, self.in_c = (b.at[k] for b in bufs)
         self.wire, self.x_first = wire, x_first
         x, y, self.core = at
         self.one, self.two = (x, y) if x_first else (y, x)
-        self.a = wire.remote(self.part.at[1 - self.core], self.in_a, peers[2])
-        self.b = wire.remote(self.to_b, self.in_b, peers[0 if x_first else 1])
-        self.c = wire.remote(self.to_c, self.in_c, peers[1 if x_first else 0])
+        if slots is None:
+            slot = [None] * 3
+        else:
+            slot = [slots[0] + 3 * k + i for i in range(3)]
+        self.a = wire.remote(self.part.at[1 - self.core], self.in_a, peers[2], slot[0])
+        self.b = wire.remote(self.to_b, self.in_b, peers[0 if x_first else 1], slot[1])
+        self.c = wire.remote(self.to_c, self.in_c, peers[1 if x_first else 0], slot[2])
 
     def pair(self, one, two):
         i, j = (one, two) if self.x_first else (two, one)
@@ -222,8 +226,8 @@
     gd_in, gd_relay, gu_in, gu_relay, swap_out, swap_in, lh, act_l, lh_sum,
     *rest,
 ):
-    eg_bufs, out_bufs = rest[:6], rest[6:12]
-    eg_fin, out_fin, gd_fin, gu_fin, send, recv, local = rest[12:]
+    eg_bufs, tail_bufs, out_bufs = rest[:6], rest[6:12], rest[12:18]
+    send, recv, local = rest[18:]
     fs, tp = lax.axis_index("fs"), lax.axis_index("tp")
     z, y = fs // 2, fs % 2
     x, c = tp // 2, tp % 2
@@ -267,8 +271,8 @@
     own_down = wire.copy(down, down_full.at[pl.ds(pl.multiple_of(z * hb, hb), hb)])
     own_e = wire.copy(earlier_in, e_all.at[half_of(y)])
     own_x = wire.copy(later_in, x_all.at[rows_of(y, tp)])
-    own_up_sum = wire.copy(up_sum, gu_fin)
-    own_down_sum = wire.copy(down_sum, gd_fin)
+    own_up_sum = wire.copy(up_sum, gu_o)
+    own_down_sum = wire.copy(down_sum, gd_o)
     scale = float(group * 2 * n) ** (-0.5)
 
     pl.semaphore_wait(barrier, 3 + (z > 0).astype(jnp.int32) + (z < n - 1).astype(jnp.int32))
@@ -304,22 +308,30 @@
     up_y = [
         wire.remote(up.at[:, cols(i, 1 - y)], up_full.at[my_rows, strip(i)], py) for i in range(n)
     ]
+    far = jnp.where(z < n // 2, n - 1, 0)
+    strips = [lax.rem(far + i, n) for i in range(n)]
+
+    def strip_at(i):
+        return pl.ds(pl.multiple_of(strips[i] * hb, hb), hb)
+
     h_y = [
-        wire.remote(hidden.at[:, cols(i, 1 - y)], h_all.at[half_of(y), strip(i)], py)
+        wire.remote(hidden.at[:, cols(strips[i], 1 - y)], h_all.at[half_of(y), strip_at(i)], py)
         for i in range(n)
     ]
 
     gds = Sums(wire, gd_part, gd_in, gd_relay, hb, 1 - y, z, n, left, right)
     gus = Sums(wire, gu_part, gu_in, gu_relay, chunk, 1 - y, z, n, left, right)
     at, peers = (x, y, c), (px, py, pc)
-    egs = [Plane(wire, eg_bufs, k, at, peers, k >= n - 1) for k in range(n)]
+    egs = [Plane(wire, eg_bufs, k, at, peers, False) for k in range(n - 1)]
+    slots = [wire.slot() for _ in range(6)]
+    tails = [
+        Plane(wire, tail_bufs, lax.rem(y + p, 2), at, peers, True, slots) for p in (0, 1)
+    ]
     outs = [Plane(wire, out_bufs, k, at, peers, True) for k in range(2 * n)]
     tile = min(256, chunk)
     slope_rows = min(256, 2 * group)
-    theirs, ours = half_of(1 - y), half_of(y)
-    lh_y = [wire.remote(lh.at[theirs, strip(i)], lh_o.at[:, cols(i, y)], py) for i in range(n)]
+    lh_y = [wire.remote(lh.at[:, strip(i)], lh_o.at[:, cols(i, y)], py) for i in range(n)]
     swap = wire.remote(swap_out, swap_in, py)
-    stores = []
 
     def start(*copies):
         for copy in copies:
@@ -329,10 +341,10 @@
         for copy in copies:
             copy.wait_recv()
 
-    def activate(parity):
-        def body(i):
-            rows = rows_of(parity, i)
-            act_t[:, rows] = squared(h_all[rows, :]).T
+    def activate(parity, i):
+        def body(j):
+            rows = rows_of(parity, j)
+            act_t[strip_at(i), rows] = squared(h_all[rows, strip_at(i)]).T
 
         loop(group // block, body)
 
@@ -347,8 +359,6 @@
         for q in range(4):
             plane.part[q % 2, q // 2, parity] = value[q * block : (q + 1) * block].astype(BF16)
 
-    far = jnp.where(z < n // 2, n - 1, 0)
-
     def gd_dots(row, size):
         rows = pl.ds(pl.multiple_of(row, hb), size)
 
@@ -373,6 +383,19 @@
 
         loop(width // tile, body)
 
+    def tail_columns(p):
+        base = column_block(n - 1).start + lax.rem(y + p, 2) * up_rows
+        return pl.ds(pl.multiple_of(base, up_rows), up_rows)
+
+    def tail_chunk(p):
+        wide = tail_columns(p)
+
+        def body(parity):
+            store_part(tails[p], parity, dot(pg[half_of(parity), :], up_full[wide, :], 1, 1))
+
+        loop(2, body)
+        tails[p].begin()
+
     def eg_chunk(k):
         wide = column_block(k)
 
@@ -395,7 +418,7 @@
         outs[k].begin()
 
     def lh_early():
-        blocks = [column_block(k) for k in range(n - 1)]
+        blocks = [column_block(k) for k in range(n - 1)] + [tail_columns(0)]
 
         def body(i):
             at = pl.ds(pl.multiple_of(i * slope_rows, slope_rows), slope_rows)
@@ -407,20 +430,36 @@
         loop(2 * group // slope_rows, body)
 
     def lh_late(parity):
-        wide = column_block(n - 1)
+        wide = tail_columns(1)
 
         def body(i):
-            at = pl.ds(pl.multiple_of(parity * group + i * slope_rows, slope_rows), slope_rows)
+            base = pl.multiple_of(i * slope_rows, slope_rows)
+            at = pl.ds(pl.multiple_of(parity * group + base, slope_rows), slope_rows)
             h = (lh_sum[at, :] + dot(x_all[at, wide], up_full[wide, :])).astype(BF16)
-            lh[at, :] = h
             act_l[at, :] = squared(h)
-
-        loop(group // slope_rows, body)
+            return base, at, h
+
+        def away(i):
+            _, at, h = body(i)
+            lh[pl.ds(pl.multiple_of(i * slope_rows, slope_rows), slope_rows), :] = h
+
+        def home(i):
+            base, _, h = body(i)
+            for j in range(n):
+                lh_o[pl.ds(base, slope_rows), cols(j, y)] = h[:, j * hb : (j + 1) * hb]
+
+        return away, home
+
+    def lh_away():
+        loop(group // slope_rows, lh_late(1 - y)[0])
+
+    def lh_home():
+        loop(group // slope_rows, lh_late(y)[1])
 
     def first_sends():
         for p in (0, 1):
             downs.begin(p)
-        start(*c_y, *up_y, *h_y, *e_y, *x_y, x_own_x, x_own_c)
+        start(*c_y, h_y[0], *up_y, *h_y[1:], *e_y, *x_y, x_own_x, x_own_c)
         for copy in own_up:
             copy.wait()
         ups.begin_at(0, 0)
@@ -432,7 +471,8 @@
     def own_act():
         for copy in own_h:
             copy.wait()
-        activate(y)
+        for i in range(n):
+            activate(y, i)
 
     def all_c():
         arrive(*c_c, *c_xc)
@@ -453,15 +493,11 @@
     def lh_send():
         start(*lh_y)
 
-    def lh_store():
-        stores.extend(wire.copy(lh.at[ours, strip(i)], lh_o.at[:, cols(i, y)]) for i in range(n))
-
-    def gd_final():
+    def gd_oal():
         own_down_sum.wait()
         for p in (0, 1):
             rows = pl.ds(pl.multiple_of(gds.half(p), hb // 2), hb // 2)
-            gd_fin[rows, :] = gd_fin[rows, :] + scale * gds.total(p)
-        stores.append(wire.copy(gd_fin, gd_o))
+            gd_o[rows, :] = gd_o[rows, :] + scale * gds.total(p)
 
     def gu_away():
         swap_out[...] = gus.total(0).astype(BF16)
@@ -472,30 +508,25 @@
         total = gus.total(1)
         for i in range(n):
             kept = total[:, i * hb : (i + 1) * hb]
-            gu_fin[:, cols(i, y)] = gu_fin[:, cols(i, y)] + scale * kept
+            gu_o[:, cols(i, y)] = gu_o[:, cols(i, y)] + scale * kept
 
     def gu_store():
         arrive(swap)
         for i in range(n):
             came = swap_in[:, strip(i)].astype(F32)
-            gu_fin[:, cols(i, 1 - y)] = gu_fin[:, cols(i, 1 - y)] + scale * came
-        stores.append(wire.copy(gu_fin, gu_o))
+            gu_o[:, cols(i, 1 - y)] = gu_o[:, cols(i, 1 - y)] + scale * came
 
     def eg_store():
-        for k in range(n):
-            egs[k].last(eg_fin, column_block(k))
-        stores.append(wire.copy(eg_fin, eg_o))
+        for k in range(n - 1):
+            egs[k].last(eg_o, column_block(k))
+        for p in (0, 1):
+            tails[p].last(eg_o, tail_columns(p))
 
     def out_last(k):
-        outs[k].last(out_fin, out_columns(k))
-
-    def out_store():
-        stores.append(wire.copy(out_fin, out_o))
+        outs[k].last(out_o, out_columns(k))
 
     def close():
         arrive(*lh_y)
-        for copy in stores:
-            copy.wait()
         wire.drain()
 
     def do(name, act, *args):
@@ -522,13 +553,16 @@
         do("down21", downs.forward, r, 1)
         for p in (0, 1):
             ups.begin_at(r, p)
-    do("h_y", arrive, *h_y)
-    do("act2", activate, 1 - y)
-    for p in (0, 1):
-        do("ups1e", ups.forward, 1, p, True)
+    do("h_y0", arrive, h_y[0])
+    do("act2", activate, 1 - y, 0)
     do("c_all", all_c)
     do("gd_far", gd_dots, far * hb, hb)
     gds.seeds([n - 2])
+    do("h_y", arrive, *h_y[1:])
+    for i in range(1, n):
+        do("act2", activate, 1 - y, i)
+    for p in (0, 1):
+        do("ups1e", ups.forward, 1, p, True)
     do("gd_dots", gd_dots, jnp.where(far == 0, hb, 0), half - hb)
     do("gd_seed", gds.seeds, range(n - 3, 0, -1))
     do("e_y0", pass_on, e_y[0], e_x[0], e_c[0])
@@ -549,7 +583,6 @@
     do("e_all", all_e)
     do("gu_dots", gu_dots)
     do("gu_seed", gus.seeds, range(n - 2, -1, -1))
-    gds.seeds([0])
     do("x_y1", pass_on, x_y[1], x_x[1], x_c[1])
     do("up1_end", ups.ends, 1)
     do("eg1", eg_chunk, 1)
@@ -567,41 +600,50 @@
     do("eg1_c", egs[1].third)
     for i in (0, 1):
         do("x_x", pass_on, x_x[i], x_xc[i])
+    for m in range(n - 3, 0, -1):
+        do("gu_relay_0", gus.relay, m, 0)
+    do("up3_0", ups.ends, last, (0,))
+    do("eg3_0", tail_chunk, 0)
     do("x_all", all_x)
+    do("eg3_0b", tails[0].second)
     do("lh_early", lh_early)
+    for m in range(n - 3, 0, -1):
+        do("gu_relay_1", gus.relay, m, 1)
     for r in range(2, last):
         do("eg2_c", egs[r].third)
-    do("up3_end", ups.ends, last)
-    do("eg3", eg_chunk, last)
-    do("lh_late1", lh_late, 1 - y)
+    do("up3_1", ups.ends, last, (1,))
+    do("eg3_1", tail_chunk, 1)
+    do("lh_away", lh_away)
     do("lh_send", lh_send)
-    do("lh_late2", lh_late, y)
-    do("eg3_b", egs[last].second)
-    lh_store()
+    do("lh_home", lh_home)
+    do("eg3_1b", tails[1].second)
     do("out0", out_chunk, 0)
-    for m in range(n - 3, 0, -1):
-        do("gu_relay", relay, gus, m)
     pieces = 2 * n
     for k in range(1, pieces):
         do("out", out_chunk, k)
         do("out_b", outs[k - 1].second)
     do("out_b", outs[pieces - 1].second)
-    do("eg3_c", egs[last].third)
+    gds.seeds([0])
+    for p in (0, 1):
+        do("eg3_c", tails[p].third)
     do("out_c", outs[0].third)
     do("gu_relay0", relay, gus, 0)
-    for k in range(1, n):
+    for k in range(1, n - 1):
         do("out_c", outs[k].third)
     do("gu_away", gu_away)
     do("eg_fin", eg_store)
+    for k in range(n - 1, n + 2):
+        do("out_c", outs[k].third)
     do("gu_home", gu_home)
-    for k in range(n, pieces):
+    for k in range(n + 2, pieces):
         do("out_c", outs[k].third)
-        do("out_last", out_last, k - n)
+        do("out_last", out_last, k - n - 2)
+    for k in range(pieces - n - 2, n):
+        do("out_last", out_last, k)
     do("gu_sto", gu_store)
-    do("gd_fin", gd_final)
+    do("gd_o", gd_oal)
     for k in range(pieces - n, pieces):
         do("out_last", out_last, k)
-    do("out_fin", out_store)
     do("close", close)
 
 
@@ -610,14 +652,11 @@
     block, hb, up_rows = later_in.shape[0], down.shape[0], up.shape[0]
     half, tokens, chunk = n * hb, 2 * group, 2 * up_rows
     any_space = pl.BlockSpec(memory_space=pl.ANY)
-    shapes = (
-        jax.ShapeDtypeStruct(later_in.shape, BF16),
-        jax.ShapeDtypeStruct(hidden.shape, BF16),
-        jax.ShapeDtypeStruct(later_in.shape, BF16),
-        jax.ShapeDtypeStruct(up.shape, F32),
-        jax.ShapeDtypeStruct(down.shape, F32),
+    vm = pltpu.VMEM
+    results = (
+        vm(later_in.shape, BF16), vm(hidden.shape, BF16), vm(later_in.shape, BF16),
+        vm(up.shape, F32), vm(down.shape, F32),
     )
-    vm = pltpu.VMEM
 
     def plane(count, columns):
         leading = (2, 2, 2), (2, 2), (2,), (2,), (), ()
@@ -631,18 +670,16 @@
         vm((2, n - 1, hb, width), BF16), vm((2, max(n - 2, 1), hb, width), BF16),
         vm((2, n - 1, chunk, half), BF16), vm((2, max(n - 2, 1), chunk, half), BF16),
         vm((up_rows, half), BF16), vm((up_rows, half), BF16),
-        vm((tokens, half), BF16), vm((tokens, half), BF16), vm((tokens, half), F32),
-        *plane(n, chunk), *plane(2 * n, chunk // 2),
-        vm((block, width), BF16), vm((block, width), BF16),
-        vm((hb, width), F32), vm(up.shape, F32),
+        vm((group, half), BF16), vm((tokens, half), BF16), vm((tokens, half), F32),
+        *plane(n - 1, chunk), *plane(2, chunk // 2), *plane(2 * n, chunk // 2),
     ]
     remote_copies = 36 * n + 40
     local_copies = 3 * n + 10
     return pl.pallas_call(
         functools.partial(layer, n),
-        out_shape=shapes,
+        out_shape=results,
         in_specs=[any_space] * 8,
-        out_specs=(any_space,) * 5,
+        out_specs=(pl.BlockSpec(memory_space=vm),) * 5,
         scratch_shapes=scratch + [
             pltpu.SemaphoreType.DMA((remote_copies,)),
             pltpu.SemaphoreType.DMA((remote_copies,)),
@@ -656,37 +693,30 @@
 
 
 def hand_on(*refs):
-    count = (len(refs) - 2) // 3
-    came, gone = refs[-2:]
-    sources, results, held = refs[:count], refs[count : 2 * count], refs[2 * count : 3 * count]
-    pieces = []
-    for source, result, hold in zip(sources, results, held):
-        parts = 2 if source.dtype == F32 or source.shape[0] > LANES * 2 else 1
-        size = source.shape[0] // parts
-        for p in range(parts):
-            at, i = pl.ds(p * size, size), len(pieces)
-            read = pltpu.make_async_copy(source.at[at], hold.at[at], came.at[i])
-            write = pltpu.make_async_copy(hold.at[at], result.at[at], gone.at[i])
-            read.start()
-            pieces.append((read, write))
-    for read, write in pieces:
-        read.wait()
-        write.start()
-    for _, write in pieces:
-        write.wait()
+    count = (len(refs) - 1) // 2
+    sources, results, gone = refs[:count], refs[count : 2 * count], refs[-1]
+    copies = [
+        pltpu.make_async_copy(source, result, gone.at[i])
+        for i, (source, result) in enumerate(zip(sources, results))
+    ]
+    for copy in copies:
+        copy.start()
+    for copy in copies:
+        copy.wait()
 
 
 def handed_on(arrays):
-    any_space = pl.BlockSpec(memory_space=pl.ANY)
+    count = len(arrays)
+    held = [pltpu.with_memory_space_constraint(a, pltpu.VMEM) for a in arrays]
     return pl.pallas_call(
         hand_on,
-        out_shape=tuple(jax.ShapeDtypeStruct(a.shape, a.dtype) for a in arrays),
-        in_specs=[any_space] * len(arrays),
-        out_specs=(any_space,) * len(arrays),
-        scratch_shapes=[pltpu.VMEM(a.shape, a.dtype) for a in arrays]
-        + [pltpu.SemaphoreType.DMA((2 * len(arrays),))] * 2,
+        out_shape=tuple(pltpu.HBM(a.shape, a.dtype) for a in arrays),
+        in_specs=[pl.BlockSpec(memory_space=pltpu.VMEM)] * count,
+        out_specs=(pl.BlockSpec(memory_space=pltpu.HBM),) * count,
+        scratch_shapes=[pltpu.SemaphoreType.DMA((count,))],
+        compiler_params=pltpu.CompilerParams(vmem_limit_bytes=1 << 20),
         name="hand_on",
-    )(*arrays)
+    )(*held)
 
 
 def portable(n_fs, later_in, earlier_in, hidden, cot, up, down, up_sum, down_sum):

time: 120 us -> 114 us (0.950)
  Pallas kernels: 119 us -> 113 us
    pallas_call x2, Pallas kernels: 119 us -> 113 us  [the longest x1 111 us: fused(): pl.pallas_call(functools.partial(layer, n), out_shape=results, in_specs=[...]
where the time goes in v3:
time: 114 us
  Pallas kernels  113 us (99%)
    pallas_call x1, Pallas kernels, fused(): pl.pallas_call(functools.partial(layer, n), out_shape=results, in_specs=[...  111 us

profile of v3, /device:TPU:0, one launch (start us, length us, event | category | flops | bytes accessed | tf_op | source)
XLA Modules:
  0.0 114.0 jit_solution(5383257982400894870)
XLA Ops:
  0.6 111.3 %layer.1 = (bf16[128,2048]{1,0:T(8,128)(2,1)S(1)}, bf16[512,1024]{1,0:T(8,128)(2,1)S(1)}, bf16[128,2048]{1,0:T(8,128)(2,1)S(1)}, f32[256,1024]{1,0:T(8,128)S(1)}, f32[128,2048]{1,0:T(8,128)S(1)}) custom-call(bf16[128,2048]{1,0:T(8,128)(2,1)} %later_in.1, bf16[512,2048]{1,0:T(8,128)(2,1)} %earlier_in.1, bf16[512,1024]{1,0:T(8,128)(2,1)} %hidden.1, ...), custom_call_target="tpu_custom_call" | custom-call | tf_op jit(solution)/shard_map/layer/pallas_call | solution.py:678
  111.9 2.1 %hand_on.1 = (bf16[128,2048]{1,0:T(8,128)(2,1)}, bf16[512,1024]{1,0:T(8,128)(2,1)}, bf16[128,2048]{1,0:T(8,128)(2,1)}, f32[256,1024]{1,0:T(8,128)}, f32[128,2048]{1,0:T(8,128)}) custom-call(bf16[128,2048]{1,0:T(8,128)(2,1)S(1)} %get-tuple-element.10.refs_0_, bf16[512,1024]{1,0:T(8,128)(2,1)S(1)} %get-tuple-element.11.refs_1_, ...), custom_call_target="tpu_custom_call" | custom-call | tf_op jit(solution)/shard_map/hand_on/pallas_call | solution.py:711

commit v4 on v3

--- a/solution.py
+++ b/solution.py
@@ -11,6 +11,7 @@
 MESH = pl.DeviceIdType.MESH
 LANES = 128
 VMEM_BYTES = 62_000_000
+SENDS = 84
 
 
 def dot(a, b, ca=1, cb=0):
@@ -34,29 +35,54 @@
     return jnp.logical_and(a, b)
 
 
+class Hop:
+    def __init__(self, wire, src, dst, device, slot):
+        self.wire, self.src, self.dst, self.device, self.slot = wire, src, dst, device, slot
+
+    def made(self, place):
+        return pltpu.make_async_remote_copy(
+            src_ref=self.src, dst_ref=self.dst, send_sem=self.wire.send.at[place],
+            recv_sem=self.wire.recv.at[self.slot], device_id=self.device, device_id_type=MESH,
+        )
+
+    def wait_recv(self):
+        self.made(0).wait_recv()
+
+
 class Wire:
     def __init__(self, send, recv, local):
         self.send, self.recv, self.local = send, recv, local
         self.n_remote = self.n_local = 0
-        self.open = []
+        self.busy = [None] * send.shape[0]
 
     def slot(self):
         self.n_remote += 1
         return self.n_remote - 1
 
     def remote(self, src, dst, device, slot=None):
-        i = self.slot() if slot is None else slot
-        return pltpu.make_async_remote_copy(
-            src_ref=src, dst_ref=dst, send_sem=self.send.at[i], recv_sem=self.recv.at[i],
-            device_id=device, device_id_type=MESH,
-        )
-
-    def start(self, copy, when=None):
+        return Hop(self, src, dst, device, self.slot() if slot is None else slot)
+
+    def free(self, place):
+        copy, when, _ = self.busy[place]
+        if when is None:
+            copy.wait_send()
+        else:
+            pl.when(when)(copy.wait_send)
+        self.busy[place] = None
+
+    def settle(self, hops):
+        for place, held in enumerate(self.busy):
+            if held is not None and held[2] in hops:
+                self.free(place)
+
+    def start(self, hop, when=None):
+        place = self.busy.index(None)
+        copy = hop.made(place)
         if when is None:
             copy.start()
         else:
             pl.when(when)(copy.start)
-        self.open.append((copy, when))
+        self.busy[place] = (copy, when, hop)
 
     def copy(self, src, dst):
         i = self.n_local
@@ -66,11 +92,9 @@
         return made
 
     def drain(self):
-        for copy, when in self.open:
-            if when is None:
-                copy.wait_send()
-            else:
-                pl.when(when)(copy.wait_send)
+        for place, held in enumerate(self.busy):
+            if held is not None:
+                self.free(place)
 
 
 class Line:
@@ -226,8 +250,8 @@
     gd_in, gd_relay, gu_in, gu_relay, swap_out, swap_in, lh, act_l, lh_sum,
     *rest,
 ):
-    eg_bufs, tail_bufs, out_bufs = rest[:6], rest[6:12], rest[12:18]
-    send, recv, local = rest[18:]
+    eg_bufs, tail_bufs, out_bufs, end_bufs = (rest[i : i + 6] for i in range(0, 24, 6))
+    send, recv, local = rest[24:]
     fs, tp = lax.axis_index("fs"), lax.axis_index("tp")
     z, y = fs // 2, fs % 2
     x, c = tp // 2, tp % 2
@@ -327,7 +351,8 @@
     tails = [
         Plane(wire, tail_bufs, lax.rem(y + p, 2), at, peers, True, slots) for p in (0, 1)
     ]
-    outs = [Plane(wire, out_bufs, k, at, peers, True) for k in range(2 * n)]
+    outs = [Plane(wire, out_bufs, k, at, peers, True) for k in range(2 * n - 1)]
+    outs += [Plane(wire, end_bufs, k, at, peers, True) for k in range(2)]
     tile = min(256, chunk)
     slope_rows = min(256, 2 * group)
     lh_y = [wire.remote(lh.at[:, strip(i)], lh_o.at[:, cols(i, y)], py) for i in range(n)]
@@ -406,7 +431,9 @@
         egs[k].begin()
 
     def out_columns(k):
-        return pl.ds(k * (chunk // 2), chunk // 2)
+        wide, narrow = chunk // 2, chunk // 4
+        whole = min(k, 2 * n - 1)
+        return pl.ds(whole * wide + (k - whole) * narrow, wide if whole == k < 2 * n - 1 else narrow)
 
     def out_chunk(k):
         wide = out_columns(k)
@@ -528,6 +555,7 @@
     def close():
         arrive(*lh_y)
         wire.drain()
+        assert wire.n_remote == recv.shape[0] and wire.n_local == local.shape[0]
 
     def do(name, act, *args):
         with jax.named_scope(name):
@@ -572,6 +600,8 @@
         do("down_end", downs.ends, r)
     own_down.wait()
     do("pg", pg_dots)
+    wire.settle([*downs.right.values(), *downs.left.values(), *up_y, *h_y, x_own_x, x_own_c, x_own_xc])
+    wire.settle([*c_y, *c_x, *c_c, *c_xc])
     do("e_y1", pass_on, e_y[1], e_x[1], e_c[1])
     do("eg0", eg_chunk, 0)
     do("e_x0", pass_on, e_x[0], e_xc[0])
@@ -607,18 +637,21 @@
     do("x_all", all_x)
     do("eg3_0b", tails[0].second)
     do("lh_early", lh_early)
+    wire.settle([*e_y, *e_x, *e_c, *e_xc, *x_y, *x_x, *x_c, *x_xc, *gds.seed.values()])
+    wire.settle([h for r in range(1, last) for p in (0, 1) for h in (ups.right[r, p], ups.left[r, p])])
+    wire.settle([h for plane in egs[:last - 1] for h in (plane.a, plane.b)])
     for m in range(n - 3, 0, -1):
         do("gu_relay_1", gus.relay, m, 1)
     for r in range(2, last):
         do("eg2_c", egs[r].third)
     do("up3_1", ups.ends, last, (1,))
-    do("eg3_1", tail_chunk, 1)
     do("lh_away", lh_away)
     do("lh_send", lh_send)
+    do("eg3_1", tail_chunk, 1)
     do("lh_home", lh_home)
     do("eg3_1b", tails[1].second)
     do("out0", out_chunk, 0)
-    pieces = 2 * n
+    pieces = len(outs)
     for k in range(1, pieces):
         do("out", out_chunk, k)
         do("out_b", outs[k - 1].second)
@@ -642,7 +675,7 @@
         do("out_last", out_last, k)
     do("gu_sto", gu_store)
     do("gd_o", gd_oal)
-    for k in range(pieces - n, pieces):
+    for k in range(n, pieces):
         do("out_last", out_last, k)
     do("close", close)
 
@@ -671,17 +704,18 @@
         vm((2, n - 1, chunk, half), BF16), vm((2, max(n - 2, 1), chunk, half), BF16),
         vm((up_rows, half), BF16), vm((up_rows, half), BF16),
         vm((group, half), BF16), vm((tokens, half), BF16), vm((tokens, half), F32),
-        *plane(n - 1, chunk), *plane(2, chunk // 2), *plane(2 * n, chunk // 2),
+        *plane(n - 1, chunk), *plane(2, chunk // 2), *plane(2 * n - 1, chunk // 2),
+        *plane(2, chunk // 4),
     ]
-    remote_copies = 36 * n + 40
-    local_copies = 3 * n + 10
+    remote_copies = 16 * (n - 1) + 3 * (n - 1) + 9 * n + 37
+    local_copies = 2 * n + 6
     return pl.pallas_call(
         functools.partial(layer, n),
         out_shape=results,
         in_specs=[any_space] * 8,
         out_specs=(pl.BlockSpec(memory_space=vm),) * 5,
         scratch_shapes=scratch + [
-            pltpu.SemaphoreType.DMA((remote_copies,)),
+            pltpu.SemaphoreType.DMA((SENDS,)),
             pltpu.SemaphoreType.DMA((remote_copies,)),
             pltpu.SemaphoreType.DMA((local_copies,)),
         ],

time: 114 us -> 112 us (0.982)
    pallas_call x1, Pallas kernels: 111 us -> 110 us  [fused(): pl.pallas_call(functools.partial(layer, n), out_shape=results, in_specs=[...]
where the time goes in v4:
time: 112 us
  Pallas kernels  112 us (100%)
    pallas_call x1, Pallas kernels, fused(): pl.pallas_call(functools.partial(layer, n), out_shape=results, in_specs=[...  110 us

profile of v4, /device:TPU:0, one launch (start us, length us, event | category | flops | bytes accessed | tf_op | source)
XLA Modules:
  0.0 112.3 jit_solution(561007626342431546)
XLA Ops:
  0.6 109.6 %layer.1 = (bf16[128,2048]{1,0:T(8,128)(2,1)S(1)}, bf16[512,1024]{1,0:T(8,128)(2,1)S(1)}, bf16[128,2048]{1,0:T(8,128)(2,1)S(1)}, f32[256,1024]{1,0:T(8,128)S(1)}, f32[128,2048]{1,0:T(8,128)S(1)}) custom-call(bf16[128,2048]{1,0:T(8,128)(2,1)} %later_in.1, bf16[512,2048]{1,0:T(8,128)(2,1)} %earlier_in.1, bf16[512,1024]{1,0:T(8,128)(2,1)} %hidden.1, ...), custom_call_target="tpu_custom_call" | custom-call | tf_op jit(solution)/shard_map/layer/pallas_call | solution.py:712
  110.2 2.1 %hand_on.1 = (bf16[128,2048]{1,0:T(8,128)(2,1)}, bf16[512,1024]{1,0:T(8,128)(2,1)}, bf16[128,2048]{1,0:T(8,128)(2,1)}, f32[256,1024]{1,0:T(8,128)}, f32[128,2048]{1,0:T(8,128)}) custom-call(bf16[128,2048]{1,0:T(8,128)(2,1)S(1)} %get-tuple-element.10.refs_0_, bf16[512,1024]{1,0:T(8,128)(2,1)S(1)} %get-tuple-element.11.refs_1_, ...), custom_call_target="tpu_custom_call" | custom-call | tf_op jit(solution)/shard_map/hand_on/pallas_call | solution.py:745

commit v5 on v4

--- a/solution.py
+++ b/solution.py
@@ -11,7 +11,7 @@
 MESH = pl.DeviceIdType.MESH
 LANES = 128
 VMEM_BYTES = 62_000_000
-SENDS = 84
+SENDS = 63
 
 
 def dot(a, b, ca=1, cb=0):
@@ -301,7 +301,10 @@
 
     pl.semaphore_wait(barrier, 3 + (z > 0).astype(jnp.int32) + (z < n - 1).astype(jnp.int32))
 
-    def spread(whole, source, first, parts):
+    def together(ref, slot):
+        Hop(wire, ref, ref, pc, slot).wait_recv()
+
+    def spread(whole, source, first, parts, shared):
         size = block // parts
 
         def sub(parity, q, i):
@@ -315,22 +318,24 @@
             src = source.at[pl.ds(pl.multiple_of(first + i * size, size), size)]
             made.append((
                 wire.remote(src, there, py), wire.remote(came, came, px),
-                wire.remote(came, came, pc), wire.remote(beside, beside, pc),
+                wire.remote(came, came, pc, shared), wire.remote(beside, beside, pc, shared),
             ))
         return zip(*made)
 
     downs = Line(wire, down_full, hb, down, y, z, n, left, right)
     ups = Line(wire, up_full, chunk, None, y, z, n, left, right)
-    c_y, c_x, c_c, c_xc = spread(c_all, cot, tp * block, 2)
-    e_y, e_x, e_c, e_xc = spread(e_all, earlier_in, tp * block, 2)
-    x_y, x_x, x_c, x_xc = spread(x_all, later_in, 0, 2)
+    c_slot, e_slot, x_slot, up_slot, h_slot, lh_slot = (wire.slot() for _ in range(6))
+    c_y, c_x, c_c, c_xc = spread(c_all, cot, tp * block, 2, c_slot)
+    e_y, e_x, e_c, e_xc = spread(e_all, earlier_in, tp * block, 2, e_slot)
+    x_y, x_x, x_c, x_xc = spread(x_all, later_in, 0, 2, x_slot)
     mine_x = x_all.at[rows_of(y, tp)]
     beside_x = x_all.at[rows_of(y, tp + 2 - 4 * x)]
     x_own_x = wire.remote(later_in, mine_x, px)
-    x_own_c = wire.remote(later_in, mine_x, pc)
-    x_own_xc = wire.remote(beside_x, beside_x, pc)
+    x_own_c = wire.remote(later_in, mine_x, pc, x_slot)
+    x_own_xc = wire.remote(beside_x, beside_x, pc, x_slot)
     up_y = [
-        wire.remote(up.at[:, cols(i, 1 - y)], up_full.at[my_rows, strip(i)], py) for i in range(n)
+        wire.remote(up.at[:, cols(i, 1 - y)], up_full.at[my_rows, strip(i)], py, up_slot)
+        for i in range(n)
     ]
     far = jnp.where(z < n // 2, n - 1, 0)
     strips = [lax.rem(far + i, n) for i in range(n)]
@@ -339,7 +344,10 @@
         return pl.ds(pl.multiple_of(strips[i] * hb, hb), hb)
 
     h_y = [
-        wire.remote(hidden.at[:, cols(strips[i], 1 - y)], h_all.at[half_of(y), strip_at(i)], py)
+        wire.remote(
+            hidden.at[:, cols(strips[i], 1 - y)], h_all.at[half_of(y), strip_at(i)], py,
+            h_slot if i else None,
+        )
         for i in range(n)
     ]
 
@@ -355,7 +363,9 @@
     outs += [Plane(wire, end_bufs, k, at, peers, True) for k in range(2)]
     tile = min(256, chunk)
     slope_rows = min(256, 2 * group)
-    lh_y = [wire.remote(lh.at[:, strip(i)], lh_o.at[:, cols(i, y)], py) for i in range(n)]
+    lh_y = [
+        wire.remote(lh.at[:, strip(i)], lh_o.at[:, cols(i, y)], py, lh_slot) for i in range(n)
+    ]
     swap = wire.remote(swap_out, swap_in, py)
 
     def start(*copies):
@@ -502,15 +512,15 @@
             activate(y, i)
 
     def all_c():
-        arrive(*c_c, *c_xc)
+        together(c_all.at[pl.ds(0, 2 * block)], c_slot)
         own_c.wait()
 
     def all_e():
-        arrive(*e_c, *e_xc)
+        together(e_all.at[pl.ds(0, 2 * block)], e_slot)
         own_e.wait()
 
     def all_x():
-        arrive(x_own_c, x_own_xc, *x_c, *x_xc)
+        together(x_all.at[pl.ds(0, 4 * block)], x_slot)
         own_x.wait()
 
     def pass_on(came, *onward):
@@ -553,7 +563,7 @@
         outs[k].last(out_o, out_columns(k))
 
     def close():
-        arrive(*lh_y)
+        together(lh_o.at[:, pl.ds(0, half)], lh_slot)
         wire.drain()
         assert wire.n_remote == recv.shape[0] and wire.n_local == local.shape[0]
 
@@ -570,7 +580,7 @@
     do("down11", downs.forward, 1, 1)
     ups.begin_at(1, 0)
     do("x_own_x", pass_on, x_own_x, x_own_xc)
-    do("up_y", arrive, *up_y)
+    do("up_y", together, up_full.at[pl.ds(0, up_rows)], up_slot)
     for stage in (0, 1):
         ups.begin_at(stage, 1)
     for r in range(2, last):
@@ -585,8 +595,10 @@
     do("act2", activate, 1 - y, 0)
     do("c_all", all_c)
     do("gd_far", gd_dots, far * hb, hb)
+    wire.settle([*c_y, *c_x, *c_c, *c_xc, *up_y, h_y[0], x_own_x, x_own_c, x_own_xc])
+    wire.settle([hop for p in (0, 1) for hop in (downs.right[1, p], downs.left[1, p])])
     gds.seeds([n - 2])
-    do("h_y", arrive, *h_y[1:])
+    do("h_y", together, h_all.at[pl.ds(0, group), pl.ds(0, half - hb)], h_slot)
     for i in range(1, n):
         do("act2", activate, 1 - y, i)
     for p in (0, 1):
@@ -600,8 +612,7 @@
         do("down_end", downs.ends, r)
     own_down.wait()
     do("pg", pg_dots)
-    wire.settle([*downs.right.values(), *downs.left.values(), *up_y, *h_y, x_own_x, x_own_c, x_own_xc])
-    wire.settle([*c_y, *c_x, *c_c, *c_xc])
+    wire.settle([*downs.right.values(), *downs.left.values(), *h_y])
     do("e_y1", pass_on, e_y[1], e_x[1], e_c[1])
     do("eg0", eg_chunk, 0)
     do("e_x0", pass_on, e_x[0], e_xc[0])
@@ -612,6 +623,8 @@
     do("e_x1", pass_on, e_x[1], e_xc[1])
     do("e_all", all_e)
     do("gu_dots", gu_dots)
+    wire.settle([*e_y, *e_x, *e_c, *e_xc, egs[0].a])
+    wire.settle([hop for p in (0, 1) for hop in (ups.right[1, p], ups.left[1, p])])
     do("gu_seed", gus.seeds, range(n - 2, -1, -1))
     do("x_y1", pass_on, x_y[1], x_x[1], x_c[1])
     do("up1_end", ups.ends, 1)
@@ -655,6 +668,7 @@
     for k in range(1, pieces):
         do("out", out_chunk, k)
         do("out_b", outs[k - 1].second)
+        wire.settle([tails[0].a, tails[1].a, *(plane.a for plane in outs[: k - 1])])
     do("out_b", outs[pieces - 1].second)
     gds.seeds([0])
     for p in (0, 1):
@@ -663,6 +677,9 @@
     do("gu_relay0", relay, gus, 0)
     for k in range(1, n - 1):
         do("out_c", outs[k].third)
+    wire.settle([*ups.right.values(), *ups.left.values(), *(h for e in egs for h in (e.a, e.b, e.c))])
+    wire.settle([gus.seed[w, m, p] for w in (0, 1) for m in range(1, n - 1) for p in (0, 1)])
+    wire.settle([tails[0].b, tails[1].b, outs[0].b, outs[1].b, *gds.pass_on.values()])
     do("gu_away", gu_away)
     do("eg_fin", eg_store)
     for k in range(n - 1, n + 2):
@@ -707,7 +724,7 @@
         *plane(n - 1, chunk), *plane(2, chunk // 2), *plane(2 * n - 1, chunk // 2),
         *plane(2, chunk // 4),
     ]
-    remote_copies = 16 * (n - 1) + 3 * (n - 1) + 9 * n + 37
+    remote_copies = 19 * (n - 1) + 6 * n + 30
     local_copies = 2 * n + 6
     return pl.pallas_call(
         functools.partial(layer, n),

time: 112 us -> 112 us (level)
  no operation moved by 1% of the time
where the time goes in v5:
time: 112 us
  Pallas kernels  111 us (99%)
    pallas_call x1, Pallas kernels, fused(): pl.pallas_call(functools.partial(layer, n), out_shape=results, in_specs=[...  109 us

profile of v5, /device:TPU:0, one launch (start us, length us, event | category | flops | bytes accessed | tf_op | source)
XLA Modules:
  0.0 111.9 jit_solution(15516687138471612049)
XLA Ops:
  0.6 109.2 %layer.1 = (bf16[128,2048]{1,0:T(8,128)(2,1)S(1)}, bf16[512,1024]{1,0:T(8,128)(2,1)S(1)}, bf16[128,2048]{1,0:T(8,128)(2,1)S(1)}, f32[256,1024]{1,0:T(8,128)S(1)}, f32[128,2048]{1,0:T(8,128)S(1)}) custom-call(bf16[128,2048]{1,0:T(8,128)(2,1)} %later_in.1, bf16[512,2048]{1,0:T(8,128)(2,1)} %earlier_in.1, bf16[512,1024]{1,0:T(8,128)(2,1)} %hidden.1, ...), custom_call_target="tpu_custom_call" | custom-call | tf_op jit(solution)/shard_map/layer/pallas_call | solution.py:729
  109.8 2.1 %hand_on.1 = (bf16[128,2048]{1,0:T(8,128)(2,1)}, bf16[512,1024]{1,0:T(8,128)(2,1)}, bf16[128,2048]{1,0:T(8,128)(2,1)}, f32[256,1024]{1,0:T(8,128)}, f32[128,2048]{1,0:T(8,128)}) custom-call(bf16[128,2048]{1,0:T(8,128)(2,1)S(1)} %get-tuple-element.10.refs_0_, bf16[512,1024]{1,0:T(8,128)(2,1)S(1)} %get-tuple-element.11.refs_1_, ...), custom_call_target="tpu_custom_call" | custom-call | tf_op jit(solution)/shard_map/hand_on/pallas_call | solution.py:762

commit v6 on v5

--- a/solution.py
+++ b/solution.py
@@ -288,11 +288,17 @@
     pl.when(z > 0)(lambda: greet(left))
     pl.when(z < n - 1)(lambda: greet(right))
 
+    def own_quarter(i):
+        q = lax.rem(tp + i, 4)
+        src = cot.at[pl.ds(pl.multiple_of(q * block, block), block)]
+        return wire.copy(src, c_all.at[rows_of(y, q)])
+
+    own_c = [own_quarter(0)]
+    own_down = wire.copy(down, down_full.at[pl.ds(pl.multiple_of(z * hb, hb), hb)])
+    own_c += [own_quarter(i) for i in range(1, 4)]
     own_h = [wire.copy(hidden.at[:, cols(i, y)], h_all.at[half_of(y), strip(i)]) for i in range(n)]
     my_rows = pl.ds(pl.multiple_of(fs * up_rows, up_rows), up_rows)
     own_up = [wire.copy(up.at[:, cols(i, y)], up_full.at[my_rows, strip(i)]) for i in range(n)]
-    own_c = wire.copy(cot, c_all.at[half_of(y)])
-    own_down = wire.copy(down, down_full.at[pl.ds(pl.multiple_of(z * hb, hb), hb)])
     own_e = wire.copy(earlier_in, e_all.at[half_of(y)])
     own_x = wire.copy(later_in, x_all.at[rows_of(y, tp)])
     own_up_sum = wire.copy(up_sum, gu_o)
@@ -322,10 +328,10 @@
             ))
         return zip(*made)
 
-    downs = Line(wire, down_full, hb, down, y, z, n, left, right)
+    downs = Line(wire, down_full, hb, None, y, z, n, left, right)
     ups = Line(wire, up_full, chunk, None, y, z, n, left, right)
     c_slot, e_slot, x_slot, up_slot, h_slot, lh_slot = (wire.slot() for _ in range(6))
-    c_y, c_x, c_c, c_xc = spread(c_all, cot, tp * block, 2, c_slot)
+    c_y, c_x, c_c, c_xc = spread(c_all, c_all, y * group + tp * block, 2, c_slot)
     e_y, e_x, e_c, e_xc = spread(e_all, earlier_in, tp * block, 2, e_slot)
     x_y, x_x, x_c, x_xc = spread(x_all, later_in, 0, 2, x_slot)
     mine_x = x_all.at[rows_of(y, tp)]
@@ -494,9 +500,12 @@
         loop(group // slope_rows, lh_late(y)[1])
 
     def first_sends():
+        own_c[0].wait()
+        start(*c_y)
+        own_down.wait()
         for p in (0, 1):
             downs.begin(p)
-        start(*c_y, h_y[0], *up_y, *h_y[1:], *e_y, *x_y, x_own_x, x_own_c)
+        start(h_y[0], *up_y, *h_y[1:], *e_y, *x_y, x_own_x, x_own_c)
         for copy in own_up:
             copy.wait()
         ups.begin_at(0, 0)
@@ -513,7 +522,8 @@
 
     def all_c():
         together(c_all.at[pl.ds(0, 2 * block)], c_slot)
-        own_c.wait()
+        for copy in own_c[1:]:
+            copy.wait()
 
     def all_e():
         together(e_all.at[pl.ds(0, 2 * block)], e_slot)
@@ -610,7 +620,6 @@
         do("ups1", ups.forward, 1, p, False)
     for r in range(1, n):
         do("down_end", downs.ends, r)
-    own_down.wait()
     do("pg", pg_dots)
     wire.settle([*downs.right.values(), *downs.left.values(), *h_y])
     do("e_y1", pass_on, e_y[1], e_x[1], e_c[1])
@@ -725,7 +734,7 @@
         *plane(2, chunk // 4),
     ]
     remote_copies = 19 * (n - 1) + 6 * n + 30
-    local_copies = 2 * n + 6
+    local_copies = 2 * n + 9
     return pl.pallas_call(
         functools.partial(layer, n),
         out_shape=results,

time: 112 us -> 112 us (level)
  no operation moved by 1% of the time
where the time goes in v6:
time: 112 us
  Pallas kernels  111 us (99%)
    pallas_call x1, Pallas kernels, fused(): pl.pallas_call(functools.partial(layer, n), out_shape=results, in_specs=[...  109 us

profile of v6, /device:TPU:0, one launch (start us, length us, event | category | flops | bytes accessed | tf_op | source)
XLA Modules:
  0.0 111.7 jit_solution(4193884604763806800)
XLA Ops:
  0.6 109.0 %layer.1 = (bf16[128,2048]{1,0:T(8,128)(2,1)S(1)}, bf16[512,1024]{1,0:T(8,128)(2,1)S(1)}, bf16[128,2048]{1,0:T(8,128)(2,1)S(1)}, f32[256,1024]{1,0:T(8,128)S(1)}, f32[128,2048]{1,0:T(8,128)S(1)}) custom-call(bf16[128,2048]{1,0:T(8,128)(2,1)} %later_in.1, bf16[512,2048]{1,0:T(8,128)(2,1)} %earlier_in.1, bf16[512,1024]{1,0:T(8,128)(2,1)} %hidden.1, ...), custom_call_target="tpu_custom_call" | custom-call | tf_op jit(solution)/shard_map/layer/pallas_call | solution.py:738
  109.6 2.1 %hand_on.1 = (bf16[128,2048]{1,0:T(8,128)(2,1)}, bf16[512,1024]{1,0:T(8,128)(2,1)}, bf16[128,2048]{1,0:T(8,128)(2,1)}, f32[256,1024]{1,0:T(8,128)}, f32[128,2048]{1,0:T(8,128)}) custom-call(bf16[128,2048]{1,0:T(8,128)(2,1)S(1)} %get-tuple-element.10.refs_0_, bf16[512,1024]{1,0:T(8,128)(2,1)S(1)} %get-tuple-element.11.refs_1_, ...), custom_call_target="tpu_custom_call" | custom-call | tf_op jit(solution)/shard_map/hand_on/pallas_call | solution.py:771

commit v7 on v6

--- a/solution.py
+++ b/solution.py
@@ -664,11 +664,11 @@
     wire.settle([h for plane in egs[:last - 1] for h in (plane.a, plane.b)])
     for m in range(n - 3, 0, -1):
         do("gu_relay_1", gus.relay, m, 1)
-    for r in range(2, last):
-        do("eg2_c", egs[r].third)
     do("up3_1", ups.ends, last, (1,))
     do("lh_away", lh_away)
     do("lh_send", lh_send)
+    for r in range(2, last):
+        do("eg2_c", egs[r].third)
     do("eg3_1", tail_chunk, 1)
     do("lh_home", lh_home)
     do("eg3_1b", tails[1].second)

time: 112 us -> 112 us (level)
  no operation moved by 1% of the time
where the time goes in v7:
time: 112 us
  Pallas kernels  111 us (99%)
    pallas_call x1, Pallas kernels, fused(): pl.pallas_call(functools.partial(layer, n), out_shape=results, in_specs=[...  109 us

profile of v7, /device:TPU:0, one launch (start us, length us, event | category | flops | bytes accessed | tf_op | source)
XLA Modules:
  0.0 111.7 jit_solution(4823022792465928872)
XLA Ops:
  0.6 109.0 %layer.1 = (bf16[128,2048]{1,0:T(8,128)(2,1)S(1)}, bf16[512,1024]{1,0:T(8,128)(2,1)S(1)}, bf16[128,2048]{1,0:T(8,128)(2,1)S(1)}, f32[256,1024]{1,0:T(8,128)S(1)}, f32[128,2048]{1,0:T(8,128)S(1)}) custom-call(bf16[128,2048]{1,0:T(8,128)(2,1)} %later_in.1, bf16[512,2048]{1,0:T(8,128)(2,1)} %earlier_in.1, bf16[512,1024]{1,0:T(8,128)(2,1)} %hidden.1, ...), custom_call_target="tpu_custom_call" | custom-call | tf_op jit(solution)/shard_map/layer/pallas_call | solution.py:738
  109.7 2.1 %hand_on.1 = (bf16[128,2048]{1,0:T(8,128)(2,1)}, bf16[512,1024]{1,0:T(8,128)(2,1)}, bf16[128,2048]{1,0:T(8,128)(2,1)}, f32[256,1024]{1,0:T(8,128)}, f32[128,2048]{1,0:T(8,128)}) custom-call(bf16[128,2048]{1,0:T(8,128)(2,1)S(1)} %get-tuple-element.10.refs_0_, bf16[512,1024]{1,0:T(8,128)(2,1)S(1)} %get-tuple-element.11.refs_1_, ...), custom_call_target="tpu_custom_call" | custom-call | tf_op jit(solution)/shard_map/hand_on/pallas_call | solution.py:771
